TPU v7x, 32 devices: a whole 2x2x4 slice. The times are simulated.
32 devices in a mesh: sp: 8 (over z, y), tp: 4 (over x, core).
Axes of the slice: x: 2, y: 2, z: 4, core: 2. Of those that a mesh axis runs over, the one named last changes fastest.
Arguments:
- resid: bfloat16 [4096, 2048], P('sp', 'tp'), may hold values from -41 to 41
- queries: bfloat16 [4096, 1024], P('sp', 'tp'), may hold values from -6 to 6
- keys: bfloat16 [4096, 1024], P('sp', 'tp'), may hold values from -6 to 6
- values: bfloat16 [4096, 1024], P('sp', 'tp'), may hold values from -6 to 6
- mix_lambda: float32 [8], P('tp'), may hold values from 0.3 to 0.8
- head_gain: float32 [128], replicated, may hold values from 0.1 to 1.9
- out_weight: bfloat16 [1024, 2048], P(None, 'tp'), may hold values from -0.1875 to 0.1875
- norm_gain: float32 [2048], P('tp'), may hold values from 0.1 to 1.9
- gate_weight: bfloat16 [2048, 5632], P('sp', 'tp'), may hold values from -0.125 to 0.125
- up_weight: bfloat16 [2048, 5632], P('sp', 'tp'), may hold values from -0.125 to 0.125
- conv_weight: float32 [3, 5632], P(None, 'tp'), may hold values from -3.5 to 3.5
- conv_bias: float32 [5632], P('tp'), may hold values from -3 to 3
- down_weight: bfloat16 [5632, 2048], P('tp', 'sp'), may hold values from -0.078125 to 0.078125
Outputs:
- layer_out: bfloat16 [4096, 2048], P('sp', 'tp')
All inputs are finite; a program needn't handle non-finite values.
Results may differ from a plain program's by a relative error of at most 0.009.
Values may be sent and summed in bfloat16 or wider, within the bound.
A program may use at most 128 MiB of HBM per device.

v0:
```python
import functools
import math

import jax
import jax.numpy as jnp
from jax import lax
from jax.experimental import pallas as pl
from jax.experimental.pallas import tpu as pltpu
from jax.sharding import PartitionSpec as P

D = 2048
HD = 64
VD = 128


def with_halo(cells, sides, width):
    for axis, dim in sides:
        count = lax.axis_size(axis)
        ends = count - 1
        head = lax.slice_in_dim(cells, 0, width, axis=dim)
        tail = lax.slice_in_dim(cells, cells.shape[dim] - width, cells.shape[dim], axis=dim)
        cells = jnp.concatenate(
            [
                lax.ppermute(tail, axis, [(i, (i + 1) % count) for i in range(ends)]),
                cells,
                lax.ppermute(head, axis, [((i + 1) % count, i) for i in range(ends)]),
            ],
            axis=dim,
        )
    return cells


def on_device(
    resid,
    queries,
    keys,
    values,
    mix_lambda,
    head_gain,
    out_weight,
    norm_gain,
    gate_weight,
    up_weight,
    conv_weight,
    conv_bias,
    down_weight,
):
    length = queries.shape[0]
    heads = mix_lambda.shape[0]
    scale = HD ** (-0.5)
    query_heads = queries.reshape(length, heads, 2, HD)
    initial = (
        jnp.full((heads, 2, length), -1e30, jnp.float32),
        jnp.zeros((heads, 2, length), jnp.float32),
        jnp.zeros((heads, 2, length, VD), jnp.float32),
    )
    key_rows = lax.all_gather(keys, "sp", axis=0, tiled=True)
    value_rows = lax.all_gather(values, "sp", axis=0, tiled=True)
    count = key_rows.shape[0]
    block = math.gcd(count, 2048)
    key_blocks = key_rows.reshape(count // block, block, heads, 2, HD)
    value_blocks = value_rows.reshape(count // block, block, heads, VD)

    def advance(state, blocks):
        running, totals, weighted = state
        key_block, value_block = blocks
        scores = (
            jnp.einsum(
                "qhmd,khmd->hmqk", query_heads, key_block, preferred_element_type=jnp.float32
            )
            * scale
        )
        highest = jnp.maximum(running, jnp.max(scores, axis=-1))
        factor = jnp.exp(running - highest)
        shifted = jnp.exp(scores - highest[..., None])
        totals = totals * factor + jnp.sum(shifted, axis=-1)
        weighted = weighted * factor[..., None] + jnp.einsum(
            "hmqk,khe->hmqe",
            shifted.astype(jnp.bfloat16),
            value_block,
            preferred_element_type=jnp.float32,
        )
        return ((highest, totals, weighted), None)

    result, unused = lax.scan(advance, initial, (key_blocks, value_blocks))
    running, totals, weighted = result
    mapped = weighted / totals[..., None]
    mixed = mapped[:, 0] - mix_lambda[:, None, None] * mapped[:, 1]
    spread = jnp.mean(mixed * mixed, axis=-1, keepdims=True)
    normed = mixed * lax.rsqrt(spread + 1e-06) * head_gain * 0.8
    heads_out = jnp.transpose(normed, (1, 0, 2)).reshape(length, heads * VD).astype(jnp.bfloat16)
    projected = jnp.dot(
        lax.all_gather(heads_out, "tp", axis=1, tiled=True),
        out_weight,
        preferred_element_type=jnp.float32,
    )
    after_mixer = resid.astype(jnp.float32) + projected
    squares = lax.psum(jnp.sum(after_mixer * after_mixer, axis=1), "tp")
    normed_rows = (after_mixer * lax.rsqrt(squares / D + 1e-06)[:, None] * norm_gain).astype(
        jnp.bfloat16
    )
    full_rows = lax.all_gather(normed_rows, "tp", axis=1, tiled=True)
    gate_sum = jnp.dot(
        full_rows,
        lax.all_gather(gate_weight, "sp", axis=0, tiled=True),
        preferred_element_type=jnp.float32,
    )
    upward = jnp.dot(
        full_rows,
        lax.all_gather(up_weight, "sp", axis=0, tiled=True),
        preferred_element_type=jnp.float32,
    )
    gated = gate_sum.astype(jnp.bfloat16)
    padded = with_halo(gated, (("sp", 0),), 1).astype(jnp.float32)
    conv = (
        padded[:-2] * conv_weight[0]
        + padded[1:-1] * conv_weight[1]
        + padded[2:] * conv_weight[2]
        + conv_bias
    )
    hidden = (jax.nn.silu(conv) * upward).astype(jnp.bfloat16)
    partial_terms = jnp.dot(
        hidden,
        lax.all_gather(down_weight, "sp", axis=1, tiled=True),
        preferred_element_type=jnp.float32,
    )
    mixer_out = lax.psum_scatter(
        partial_terms.astype(jnp.bfloat16), "tp", scatter_dimension=1, tiled=True
    ).astype(jnp.float32)
    return (after_mixer + mixer_out).astype(jnp.bfloat16)


PAIR, LINE = 0, 1
EDGE = 16


def layer_kernel(
    sp,
    tp,
    resid,
    queries,
    keys,
    values,
    mix_lambda,
    head_gain,
    out_weight,
    norm_gain,
    gate_weight,
    up_weight,
    conv_weight,
    conv_bias,
    down_weight,
    out,
    kv,
    gates,
    ups,
    downs,
    peaks,
    totals,
    weighted,
    heads_all,
    after,
    square_all,
    rows_all,
    gate_acc,
    up_acc,
    hidden,
    partials,
    landed,
    local_sem,
    kv_send,
    kv_recv,
    w_send,
    w_recv,
    head_send,
    head_recv,
    square_send,
    square_recv,
    row_send,
    row_recv,
    edge_send,
    edge_recv,
    part_send,
    part_recv,
):
    bf16, f32 = jnp.bfloat16, jnp.float32
    me = lax.axis_index("sp")
    t = lax.axis_index("tp")
    nz = sp // 2
    z, y = me // 2, lax.rem(me, 2)
    length = queries.shape[0]
    heads = queries.shape[1] // VD
    half_k = gate_weight.shape[0] // 2
    half_f = down_weight.shape[0] // 2
    weights = (gates, ups, downs)

    local = [
        pltpu.make_async_copy(keys, kv.at[me, 0], local_sem.at[0]),
        pltpu.make_async_copy(values, kv.at[me, 1], local_sem.at[1]),
    ]
    for i, ref in enumerate((gate_weight, up_weight)):
        for h in range(2):
            local.append(
                pltpu.make_async_copy(
                    ref.at[pl.ds(h * half_k, half_k)],
                    weights[i].at[me, h],
                    local_sem.at[2 + 2 * i + h],
                )
            )
    for h in range(2):
        local.append(
            pltpu.make_async_copy(
                down_weight.at[pl.ds(h * half_f, half_f)], downs.at[me, h], local_sem.at[6 + h]
            )
        )
    for copy in local:
        copy.start()

    def routes(kind, zs, ys):
        if kind == PAIR:
            up = jnp.logical_and(zs <= z, z < nz - 1)
            down = jnp.logical_and(zs >= z, z > 0)
            across = jnp.logical_and(zs == z, ys == y)
        else:
            up = jnp.logical_and(ys == y, jnp.logical_and(zs <= z, z < nz - 1))
            down = jnp.logical_and(ys == y, jnp.logical_and(zs >= z, z > 0))
            across = ys == y
        return (
            (up, jnp.minimum(me + 2, sp - 1)),
            (down, jnp.maximum(me - 2, 0)),
            (across, 2 * z + 1 - y),
        )

    def remote(ref, send, recv, target):
        return pltpu.make_async_remote_copy(
            src_ref=ref,
            dst_ref=ref,
            send_sem=send,
            recv_sem=recv,
            device_id={"sp": target},
            device_id_type=pl.DeviceIdType.MESH,
        )

    def kv_copy(kind, src, way, target):
        return remote(kv.at[src, kind], kv_send.at[kind, way, src], kv_recv.at[kind, src], target)

    def w_copy(array, kind, src, way, target):
        return remote(
            weights[array].at[src, kind],
            w_send.at[array, kind, way, src],
            w_recv.at[array, kind, src],
            target,
        )

    def push(make, kind, src, ways=(0, 1, 2), wait=False):
        zs, ys = src // 2, lax.rem(src, 2)
        plan = routes(kind, zs, ys)
        for way in ways:
            needed, target = plan[way]

            @pl.when(needed)
            def _():
                copy = make(kind, src, way, target)
                if wait:
                    copy.wait_send()
                else:
                    copy.start()

    def take(make, kind, src):
        @pl.when(src != me)
        def _():
            make(kind, src, 0, lax.rem(me + 2, sp)).wait_recv()
            push(make, kind, src)

    def visit(first, last, body, after_ring=None):
        def event(e, carry):
            d = e // 4
            above = lax.rem(e, 2)
            ys = lax.rem(y + lax.rem(e // 2, 2), 2)
            zs = jnp.where(above == 1, z + d, z - d)
            valid = jnp.logical_and(jnp.logical_and(zs >= 0, zs < nz), d + (1 - above) > 0)

            @pl.when(valid)
            def _():
                body(2 * zs + ys)

            if after_ring is not None:

                @pl.when(lax.rem(e, 4) == 3)
                def _():
                    after_ring(d)

            return carry

        lax.fori_loop(4 * first, 4 * last, event, 0)

    for copy in local:
        copy.wait()
    push(kv_copy, PAIR, me)
    push(kv_copy, LINE, me)

    peaks[...] = jnp.full(peaks.shape, -1e30, f32)
    totals[...] = jnp.zeros(totals.shape, f32)
    weighted[...] = jnp.zeros(weighted.shape, f32)
    lanes = lax.broadcasted_iota(jnp.int32, (1, 2 * HD), 1)
    scale = HD**-0.5
    rows = math.gcd(length, 256)

    def attend(src):
        take(kv_copy, PAIR, src)
        take(kv_copy, LINE, src)

        def row_block(r, carry):
            at = pl.ds(pl.multiple_of(r * rows, rows), rows)
            for h in range(heads):
                cols = slice(h * VD, (h + 1) * VD)
                q = queries[at, cols].astype(f32) * scale
                key_block = kv[src, 0, :, cols]
                value_block = kv[src, 1, :, cols]
                for m in range(2):
                    keep = lanes < HD if m == 0 else lanes >= HD
                    qm = jnp.where(keep, q, 0.0).astype(bf16)
                    s = lax.dot_general(
                        qm, key_block, (((1,), (1,)), ((), ())), preferred_element_type=f32
                    )
                    i = 2 * h + m
                    old = peaks[i, at, :]
                    new = jnp.maximum(old, jnp.max(s, axis=1, keepdims=True))
                    factor = jnp.exp(old - new)
                    p = jnp.exp(s - new)
                    peaks[i, at, :] = new
                    totals[i, at, :] = totals[i, at, :] * factor + jnp.sum(
                        p, axis=1, keepdims=True
                    )
                    weighted[i, at, :] = weighted[i, at, :] * factor + jnp.dot(
                        p.astype(bf16), value_block, preferred_element_type=f32
                    )
            return carry

        lax.fori_loop(0, length // rows, row_block, 0)

    def feed(d):
        for way, turn in ((0, z), (1, nz - 1 - z), (2, nz - 1)):

            @pl.when(d == turn)
            def _():
                for array in range(3):
                    for kind in (PAIR, LINE):
                        push(functools.partial(w_copy, array), kind, me, (way,))

    visit(0, nz, attend, feed)

    for h in range(heads):
        first = weighted[2 * h] / totals[2 * h]
        second = weighted[2 * h + 1] / totals[2 * h + 1]
        mixed = first - mix_lambda[h] * second
        spread = jnp.mean(mixed * mixed, axis=1, keepdims=True)
        normed = mixed * lax.rsqrt(spread + 1e-06) * head_gain[...] * 0.8
        heads_all[t, :, h * VD : (h + 1) * VD] = normed.astype(bf16)

    core = lax.rem(t, 2)
    sibling = t + 1 - 2 * core
    half_tp = tp // 2

    def tp_copy(ref, send, recv, target):
        return pltpu.make_async_remote_copy(
            src_ref=ref,
            dst_ref=ref,
            send_sem=send,
            recv_sem=recv,
            device_id={"tp": target},
            device_id_type=pl.DeviceIdType.MESH,
        )

    def spread(slot, send, recv):
        copies = []
        for k in range(1, half_tp):
            copies.append(tp_copy(slot(t), send.at[k], recv.at[k], lax.rem(t + 2 * k, tp)))
            copies[-1].start()
        copies.append(tp_copy(slot(t), send.at[0], recv.at[0], sibling))
        copies[-1].start()
        return copies

    def settle(slot, send, recv, copies):
        for k in range(1, half_tp):
            copies[k - 1].wait_recv()
            came = lax.rem(t + tp - 2 * k, tp)
            copies.append(
                tp_copy(slot(came), send.at[half_tp + k], recv.at[half_tp + k], sibling)
            )
            copies[-1].start()
        for copy in copies[half_tp - 1 :]:
            copy.wait_recv()
        for copy in copies:
            copy.wait_send()

    def exchange(slot, send, recv):
        settle(slot, send, recv, spread(slot, send, recv))

    exchange(lambda j: heads_all.at[j], head_send, head_recv)
    width = heads * VD
    total = resid[...].astype(f32)
    for j in range(tp):
        total = total + jnp.dot(
            heads_all[j], out_weight[j * width : (j + 1) * width, :], preferred_element_type=f32
        )
    after[...] = total
    row_sum = jnp.sum(total * total, axis=1, keepdims=True)
    square_all[t] = jnp.transpose(jnp.broadcast_to(row_sum, (length, 128)))[:8]
    exchange(lambda j: square_all.at[j], square_send, square_recv)
    summed = square_all[0]
    for j in range(1, tp):
        summed = summed + square_all[j]
    inverse = lax.rsqrt(summed / D + 1e-06)
    inverse = jnp.transpose(jnp.concatenate([inverse] * 16, axis=0))[:, :1]
    rows_all[t, EDGE : EDGE + length, :] = (after[...] * inverse * norm_gain[...]).astype(bf16)
    own_rows = lambda j: rows_all.at[j, pl.ds(EDGE, length)]
    sent = spread(own_rows, row_send, row_recv)

    def relay(src):
        for array in range(3):
            for kind in (PAIR, LINE):
                take(functools.partial(w_copy, array), kind, src)

    visit(0, 1, relay)
    settle(own_rows, row_send, row_recv, sent)

    def edge_copy(way, source, dest, target):
        return pltpu.make_async_remote_copy(
            src_ref=rows_all.at[:, pl.ds(source, EDGE)],
            dst_ref=rows_all.at[:, pl.ds(dest, EDGE)],
            send_sem=edge_send.at[way],
            recv_sem=edge_recv.at[way],
            device_id={"sp": target},
            device_id_type=pl.DeviceIdType.MESH,
        )

    onward = edge_copy(0, length, 0, jnp.minimum(me + 1, sp - 1))
    back = edge_copy(1, EDGE, EDGE + length, jnp.maximum(me - 1, 0))
    not_last, not_first = me < sp - 1, me > 0

    @pl.when(not_last)
    def _():
        onward.start()

    @pl.when(not_first)
    def _():
        back.start()

    @pl.when(me == 0)
    def _():
        rows_all[:, 0:EDGE, :] = jnp.zeros((tp, EDGE, rows_all.shape[2]), bf16)

    @pl.when(me == sp - 1)
    def _():
        rows_all[:, EDGE + length :, :] = jnp.zeros((tp, EDGE, rows_all.shape[2]), bf16)

    visit(1, 2, relay)

    @pl.when(not_first)
    def _():
        onward.wait_recv()

    @pl.when(not_last)
    def _():
        back.wait_recv()

    gate_acc[...] = jnp.zeros(gate_acc.shape, f32)
    up_acc[...] = jnp.zeros(up_acc.shape, f32)
    per = sp // tp
    depth = 2 * half_k
    ff = gate_weight.shape[1]

    def expand(src):
        cols = pl.ds(pl.multiple_of(lax.rem(src, per) * depth, depth), depth)
        x = rows_all[src // per, :, cols]
        gate_acc[...] += jnp.dot(
            x, gates[src].reshape(depth, ff), preferred_element_type=f32
        )
        up_acc[...] += jnp.dot(
            x[EDGE : EDGE + length], ups[src].reshape(depth, ff), preferred_element_type=f32
        )

    def relay_expand(src):
        relay(src)
        expand(src)

    visit(0, 2, expand)
    visit(2, nz, relay_expand)

    for c in range(0, ff, 128):
        cols = slice(c, c + 128)

        def tap(start):
            return gate_acc[start : start + length, cols].astype(bf16).astype(f32)

        conv = (
            tap(EDGE - 1) * conv_weight[0:1, cols]
            + tap(EDGE) * conv_weight[1:2, cols]
            + tap(EDGE + 1) * conv_weight[2:3, cols]
            + conv_bias[:, cols]
        )
        hidden[:, cols] = (conv / (1.0 + jnp.exp(-conv)) * up_acc[:, cols]).astype(bf16)

    def part(owner, q):
        return jnp.dot(
            hidden[...],
            downs[owner * per + q].reshape(2 * half_f, downs.shape[3]),
            preferred_element_type=f32,
        )

    def part_copy(slot, q, target):
        return pltpu.make_async_remote_copy(
            src_ref=partials.at[slot, q],
            dst_ref=landed.at[slot, q],
            send_sem=part_send.at[slot, q],
            recv_sem=part_recv.at[slot, q],
            device_id={"tp": target},
            device_id_type=pl.DeviceIdType.MESH,
        )

    shipped = []
    for k in range(1, half_tp):
        chip = lax.rem(t // 2 + k, half_tp)
        for q in range(per):
            partials[half_tp + k, q] = part(2 * chip + 1 - core, q).astype(bf16)
            copy = part_copy(half_tp + k, q, sibling)
            copy.start()
            shipped.append(copy)
        for q in range(per):
            mine = part(2 * chip + core, q)
            shipped[(k - 1) * 2 * per + q].wait_recv()
            partials[k, q] = (mine + landed[half_tp + k, q].astype(f32)).astype(bf16)
            copy = part_copy(k, q, 2 * chip + core)
            copy.start()
            shipped.append(copy)
    for q in range(per):
        partials[0, q] = part(sibling, q).astype(bf16)
        copy = part_copy(0, q, sibling)
        copy.start()
        shipped.append(copy)
    wide = partials.shape[3]
    for q in range(per):
        cols = slice(q * wide, (q + 1) * wide)
        after[:, cols] += part(t, q)
    for q in range(per):
        cols = slice(q * wide, (q + 1) * wide)
        total = after[:, cols]
        for k in range(half_tp):
            part_copy(k, q, sibling).wait_recv()
            total = total + landed[k, q].astype(f32)
        out[:, cols] = total.astype(bf16)
    for copy in shipped:
        copy.wait_send()

    @pl.when(not_last)
    def _():
        onward.wait_send()

    @pl.when(not_first)
    def _():
        back.wait_send()

    def drain(src, carry):
        for kind in (PAIR, LINE):
            push(kv_copy, kind, src, wait=True)
            for array in range(3):
                push(functools.partial(w_copy, array), kind, src, wait=True)

        return carry

    lax.fori_loop(0, sp, drain, 0)


def fused(sp, tp, *args):
    resid, queries, keys, values = args[:4]
    gate_weight, down_weight = args[8], args[12]
    length, width = queries.shape
    features = resid.shape[1]
    depth, ff = gate_weight.shape
    maps = 2 * (width // VD)
    bf16, f32 = jnp.bfloat16, jnp.float32
    dma = pltpu.SemaphoreType.DMA
    vmem = pl.BlockSpec(memory_space=pltpu.VMEM)
    smem = pl.BlockSpec(memory_space=pltpu.SMEM)
    hbm = pl.BlockSpec(memory_space=pl.ANY)
    rows = length + 2 * EDGE
    down_cols = down_weight.shape[1]
    args = list(args)
    for i in (5, 7, 11):
        args[i] = args[i].reshape(1, -1)
    return pl.pallas_call(
        functools.partial(layer_kernel, sp, tp),
        out_shape=jax.ShapeDtypeStruct(resid.shape, bf16),
        in_specs=[
            vmem, vmem, hbm, hbm, smem, vmem, vmem, vmem, hbm, hbm, vmem, vmem, hbm,
        ],
        out_specs=vmem,
        scratch_shapes=[
            pltpu.VMEM((sp, 2, length, width), bf16),
            pltpu.VMEM((sp, 2, depth // 2, ff), bf16),
            pltpu.VMEM((sp, 2, depth // 2, ff), bf16),
            pltpu.VMEM((sp, 2, ff // 2, down_cols), bf16),
            pltpu.VMEM((maps, length, 1), f32),
            pltpu.VMEM((maps, length, 1), f32),
            pltpu.VMEM((maps, length, VD), f32),
            pltpu.VMEM((tp, length, width), bf16),
            pltpu.VMEM((length, features), f32),
            pltpu.VMEM((tp, 8, length), f32),
            pltpu.VMEM((tp, rows, features), bf16),
            pltpu.VMEM((rows, ff), f32),
            pltpu.VMEM((length, ff), f32),
            pltpu.VMEM((length, ff), bf16),
            pltpu.VMEM((tp, sp // tp, length, down_cols), bf16),
            pltpu.VMEM((tp, sp // tp, length, down_cols), bf16),
            dma((8,)),
            dma((2, 3, sp)),
            dma((2, sp)),
            dma((3, 2, 3, sp)),
            dma((3, 2, sp)),
            dma((tp,)),
            dma((tp,)),
            dma((tp,)),
            dma((tp,)),
            dma((tp,)),
            dma((tp,)),
            dma((2,)),
            dma((2,)),
            dma((tp, sp // tp)),
            dma((tp, sp // tp)),
        ],
        compiler_params=pltpu.CompilerParams(
            has_side_effects=True, vmem_limit_bytes=60 * 1024 * 1024
        ),
    )(*args)


def solution(mesh):
    sp, tp = mesh.shape["sp"], mesh.shape["tp"]

    def run(*args):
        width, depth = args[1].shape[1], args[8].shape[0]
        small = args[0].shape[0] <= 512
        whole_pairs = sp % 2 == 0 and tp % 2 == 0 and sp % tp == 0
        if whole_pairs and small and depth % 256 == 0 and width % VD == 0:
            return fused(sp, tp, *args)
        return on_device(*args)


    placed = (
        P("sp", "tp"),
        P("sp", "tp"),
        P("sp", "tp"),
        P("sp", "tp"),
        P("tp"),
        P(),
        P(None, "tp"),
        P("tp"),
        P("sp", "tp"),
        P("sp", "tp"),
        P(None, "tp"),
        P("tp"),
        P("tp", "sp"),
    )
    return jax.shard_map(
        run, mesh=mesh, in_specs=placed, out_specs=P("sp", "tp"), check_vma=False
    )
```

profile of v0, /device:TPU:0, one launch (start us, length us, event | category | flops | bytes accessed | tf_op | source)
XLA Modules:
  0.0 304.7 jit_solution(16250074076778548218)
XLA Ops:
  0.0 1.3 reshape.11.conv_bias
  1.3 301.5 %shard_map.127 = bf16[512,512]{1,0:T(8,128)(2,1)} custom-call(bf16[512,512]{1,0:T(8,128)(2,1)} %resid.1, bf16[512,256]{1,0:T(8,128)(2,1)} %queries.1, bf16[512,256]{1,0:T(8,128)(2,1)} %keys.1, bf16[512,256]{1,0:T(8,128)(2,1)} %values.1, f32[2]{0:T(128)} %mix_lambda.1, f32[1,128]{1,0:T(1,128)} %bitcast.3, bf16[1024,512]{1,0:T(8,128)(2,1)} %out_weight.1, ...), custom_call_target="tpu_custom_call" | custom-call | tf_op jit(solution)/shard_map/pallas_call | solution.py:592
  302.8 1.9 copy.15
where the time goes:
time: 305 us
  Pallas kernels  302 us (99%)
  local copies, waits for them, and re-layouts  3.16 us (1%)
    pallas_call x1, Pallas kernels, fused(): pl.pallas_call(functools.partial(layer_kernel, sp, tp), out_shape=jax.Sha...  302 us

commit v1 on v0

v1 whole, which is shorter than its diff:
```python
import functools
import math

import jax
import jax.numpy as jnp
from jax import lax
from jax.experimental import pallas as pl
from jax.experimental.pallas import tpu as pltpu
from jax.sharding import PartitionSpec as P

D = 2048
HD = 64
VD = 128


def with_halo(cells, sides, width):
    for axis, dim in sides:
        count = lax.axis_size(axis)
        ends = count - 1
        head = lax.slice_in_dim(cells, 0, width, axis=dim)
        tail = lax.slice_in_dim(cells, cells.shape[dim] - width, cells.shape[dim], axis=dim)
        cells = jnp.concatenate(
            [
                lax.ppermute(tail, axis, [(i, (i + 1) % count) for i in range(ends)]),
                cells,
                lax.ppermute(head, axis, [((i + 1) % count, i) for i in range(ends)]),
            ],
            axis=dim,
        )
    return cells


def on_device(
    resid,
    queries,
    keys,
    values,
    mix_lambda,
    head_gain,
    out_weight,
    norm_gain,
    gate_weight,
    up_weight,
    conv_weight,
    conv_bias,
    down_weight,
):
    length = queries.shape[0]
    heads = mix_lambda.shape[0]
    scale = HD ** (-0.5)
    query_heads = queries.reshape(length, heads, 2, HD)
    initial = (
        jnp.full((heads, 2, length), -1e30, jnp.float32),
        jnp.zeros((heads, 2, length), jnp.float32),
        jnp.zeros((heads, 2, length, VD), jnp.float32),
    )
    key_rows = lax.all_gather(keys, "sp", axis=0, tiled=True)
    value_rows = lax.all_gather(values, "sp", axis=0, tiled=True)
    count = key_rows.shape[0]
    block = math.gcd(count, 2048)
    key_blocks = key_rows.reshape(count // block, block, heads, 2, HD)
    value_blocks = value_rows.reshape(count // block, block, heads, VD)

    def advance(state, blocks):
        running, totals, weighted = state
        key_block, value_block = blocks
        scores = (
            jnp.einsum(
                "qhmd,khmd->hmqk", query_heads, key_block, preferred_element_type=jnp.float32
            )
            * scale
        )
        highest = jnp.maximum(running, jnp.max(scores, axis=-1))
        factor = jnp.exp(running - highest)
        shifted = jnp.exp(scores - highest[..., None])
        totals = totals * factor + jnp.sum(shifted, axis=-1)
        weighted = weighted * factor[..., None] + jnp.einsum(
            "hmqk,khe->hmqe",
            shifted.astype(jnp.bfloat16),
            value_block,
            preferred_element_type=jnp.float32,
        )
        return ((highest, totals, weighted), None)

    result, unused = lax.scan(advance, initial, (key_blocks, value_blocks))
    running, totals, weighted = result
    mapped = weighted / totals[..., None]
    mixed = mapped[:, 0] - mix_lambda[:, None, None] * mapped[:, 1]
    spread = jnp.mean(mixed * mixed, axis=-1, keepdims=True)
    normed = mixed * lax.rsqrt(spread + 1e-06) * head_gain * 0.8
    heads_out = jnp.transpose(normed, (1, 0, 2)).reshape(length, heads * VD).astype(jnp.bfloat16)
    projected = jnp.dot(
        lax.all_gather(heads_out, "tp", axis=1, tiled=True),
        out_weight,
        preferred_element_type=jnp.float32,
    )
    after_mixer = resid.astype(jnp.float32) + projected
    squares = lax.psum(jnp.sum(after_mixer * after_mixer, axis=1), "tp")
    normed_rows = (after_mixer * lax.rsqrt(squares / D + 1e-06)[:, None] * norm_gain).astype(
        jnp.bfloat16
    )
    full_rows = lax.all_gather(normed_rows, "tp", axis=1, tiled=True)
    gate_sum = jnp.dot(
        full_rows,
        lax.all_gather(gate_weight, "sp", axis=0, tiled=True),
        preferred_element_type=jnp.float32,
    )
    upward = jnp.dot(
        full_rows,
        lax.all_gather(up_weight, "sp", axis=0, tiled=True),
        preferred_element_type=jnp.float32,
    )
    gated = gate_sum.astype(jnp.bfloat16)
    padded = with_halo(gated, (("sp", 0),), 1).astype(jnp.float32)
    conv = (
        padded[:-2] * conv_weight[0]
        + padded[1:-1] * conv_weight[1]
        + padded[2:] * conv_weight[2]
        + conv_bias
    )
    hidden = (jax.nn.silu(conv) * upward).astype(jnp.bfloat16)
    partial_terms = jnp.dot(
        hidden,
        lax.all_gather(down_weight, "sp", axis=1, tiled=True),
        preferred_element_type=jnp.float32,
    )
    mixer_out = lax.psum_scatter(
        partial_terms.astype(jnp.bfloat16), "tp", scatter_dimension=1, tiled=True
    ).astype(jnp.float32)
    return (after_mixer + mixer_out).astype(jnp.bfloat16)


EDGE = 16
LANES = 128


def layer_kernel(
    sp,
    tp,
    resid,
    queries,
    keys,
    values,
    mix_lambda,
    head_gain,
    out_weight,
    norm_gain,
    gate_weight,
    up_weight,
    conv_weight,
    conv_bias,
    down_weight,
    out,
    q_all,
    qs,
    kv,
    gates,
    ups,
    downs,
    peaks,
    totals,
    weighted,
    heads_own,
    heads_all,
    out_all,
    resid_all,
    gain_all,
    after,
    after_own,
    rows_all,
    gate_acc,
    up_acc,
    hidden,
    held,
    stage,
    from_core,
    from_x,
    from_z,
    local_sem,
    send_sem,
    recv_sem,
    q_sem,
    head_send,
    head_recv,
    out_send,
    out_recv,
    resid_send,
    resid_recv,
    gain_send,
    gain_recv,
    row_sem,
    after_sem,
    edge_send,
    edge_recv,
    part_send,
    core_recv,
    x_recv,
    z_recv,
):
    bf16, f32 = jnp.bfloat16, jnp.float32
    div, rem = lax.div, lax.rem
    me = lax.axis_index("sp")
    t = lax.axis_index("tp")
    z, y = div(me, 2), rem(me, 2)
    h, q = div(z, 2), rem(z, 2)
    x, c = div(t, 2), rem(t, 2)
    mate = me + 2 - 4 * q
    across = me + 1 - 2 * y
    far = me + 4 - 8 * h
    fmate = far + 2 - 4 * q
    adjacent = me + 2 - 4 * h
    amate = across + 2 - 4 * q
    afar = across + 4 - 8 * h
    afmate = afar + 2 - 4 * q
    inner = h != q
    sibling = t + 1 - 2 * c
    xdev = t + 2 - 4 * x
    xsib = sibling + 2 - 4 * x

    length = queries.shape[0]
    depth, ff = gate_weight.shape
    features = resid.shape[1]
    big = gates.shape[2]
    small = ff - big
    down_cols = down_weight.shape[1]
    half_sp = sp // 2
    K, V, GATE, UP, DOWN = range(5)
    ACROSS, FAR, MATE, ADJACENT = range(4)

    drains = []

    def both(a, b):
        return b if a is None else jnp.logical_and(a, b)

    def when(cond, body):
        if cond is None:
            body()
        else:
            pl.when(cond)(body)

    def remote(src, dst, send, recv, target):
        return pltpu.make_async_remote_copy(
            src_ref=src,
            dst_ref=dst,
            send_sem=send,
            recv_sem=recv,
            device_id=target,
            device_id_type=pl.DeviceIdType.MESH,
        )

    def ship(make, cond=None):
        when(cond, lambda: make().start())
        drains.append((cond, make))

    def variants(array, part):
        if array in (K, V):
            return ((None, 0),)
        return ((c == part, big), (c != part, small))

    def landing(array, src, size):
        if array in (K, V):
            return kv.at[src, array]
        if array == DOWN:
            return downs.at[src, pl.ds(0, size)]
        return (gates, ups)[array - GATE].at[src, :, pl.ds(0, size)]

    def origin(array, part, size):
        if array in (K, V):
            cols = pl.ds(pl.multiple_of(part * VD, VD), VD)
            return (keys, values)[array].at[:, cols]
        cut = pl.ds(pl.multiple_of(part * (ff - size), LANES), size)
        if array == DOWN:
            return down_weight.at[cut]
        return (gate_weight, up_weight)[array - GATE].at[:, cut]

    def send(array, src, way, target, part=None, cond=None):
        for which, size in variants(array, q if part is None else part):

            def make(size=size):
                here = landing(array, src, size)
                return remote(
                    here if part is None else origin(array, part, size),
                    here,
                    send_sem.at[array, way, src],
                    recv_sem.at[array, src],
                    {"sp": target},
                )

            ship(make, both(cond, which) if which is not None else cond)

    def feed(array, *ways):
        other = 1 - q
        for way in ways:
            if way == ACROSS:
                send(array, me, ACROSS, across, part=q)
            elif way == FAR:
                send(array, me, FAR, far, part=q)
            elif way == MATE:
                send(array, me, MATE, mate, part=other)
            else:
                send(array, me, ADJACENT, adjacent, part=other, cond=inner)

    def arrive(array, src):
        for which, size in variants(array, q):

            def wait(size=size):
                here = landing(array, src, size)
                remote(
                    here, here, send_sem.at[array, 0, src], recv_sem.at[array, src], {"sp": across}
                ).wait_recv()

            when(which, wait)

    def pass_on(array, src, *ways):
        arrive(array, src)
        for way in ways:
            if way == FAR:
                send(array, src, FAR, far, cond=inner)
            else:
                send(array, src, ACROSS, across)

    for way in (MATE, ADJACENT, FAR, ACROSS):
        for array in (K, V):
            feed(array, way)

    def q_copy():
        cols = pl.ds(pl.multiple_of((1 - q) * VD, VD), VD)
        return remote(queries.at[:, cols], q_all.at[q], q_sem.at[0], q_sem.at[1], {"sp": mate})

    ship(q_copy)

    local = []

    def fetch(src, dst, cond=None):
        sem = local_sem.at[len(local)]
        make = lambda: pltpu.make_async_copy(src, dst, sem)
        local.append((cond, make))
        when(cond, lambda: make().start())

    def fetched(first, last=None):
        for cond, make in local[first:last]:
            when(cond, lambda: make().wait())

    own_cols = pl.ds(pl.multiple_of(q * VD, VD), VD)
    fetch(queries.at[:, own_cols], q_all.at[q])
    for array in (K, V):
        fetch(origin(array, q, 0), landing(array, me, 0))
    early = len(local)
    for array in (GATE, UP, DOWN):
        for which, size in variants(array, q):
            fetch(origin(array, q, size), landing(array, me, size), which)
    fetch(out_weight, out_all.at[t])
    fetch(resid, resid_all.at[t], c == q)
    fetch(norm_gain, gain_all.at[t])

    def out_copy(src, slot, target, send):
        return lambda: remote(
            src, out_all.at[slot], out_send.at[send], out_recv.at[slot], {"tp": target}
        )

    def gain_copy(target, send):
        return lambda: remote(
            norm_gain, gain_all.at[t], gain_send.at[send], gain_recv.at[t], {"tp": target}
        )

    def resid_copy(src, slot, target, send):
        return lambda: remote(
            src, resid_all.at[slot], resid_send.at[send], resid_recv.at[slot], target
        )

    for i, target in enumerate((sibling, xdev, xsib)):
        ship(gain_copy(target, i))
    ship(out_copy(out_weight, t, xdev, 0))
    ship(resid_copy(resid, t, {"tp": 2 * (1 - x) + q}, 0))
    ship(out_copy(out_weight, t, sibling, 1))
    ship(resid_copy(resid, t, {"tp": sibling}, 1), c != q)

    peaks[...] = jnp.full(peaks.shape, -1e30, f32)
    totals[...] = jnp.zeros(totals.shape, f32)
    weighted[...] = jnp.zeros(weighted.shape, f32)

    @pl.when(c != q)
    def _():
        downs[:, small:, :] = jnp.zeros((sp, big - small, down_cols), bf16)

    fetched(0, early)
    lanes = lax.broadcasted_iota(jnp.int32, (1, VD), 1)

    def spread_queries(block):
        value = q_all[block].astype(f32) * HD**-0.5
        at = pl.ds(pl.multiple_of(block * length, length), length)
        for m in range(2):
            keep = lanes < HD if m == 0 else lanes >= HD
            qs[m, at, :] = jnp.where(keep, value, 0.0).astype(bf16)

    rows = math.gcd(length, 256)

    def attend(src, first=0, last=2 * length // rows):
        def row_block(r, carry):
            at = pl.ds(pl.multiple_of(r * rows, rows), rows)
            key_block = kv[src, K]
            value_block = kv[src, V]
            for m in range(2):
                s = lax.dot_general(
                    qs[m, at, :], key_block, (((1,), (1,)), ((), ())), preferred_element_type=f32
                )
                old = peaks[m, at, :]
                new = jnp.maximum(old, jnp.max(s, axis=1, keepdims=True))
                factor = jnp.exp(old - new)
                p = jnp.exp(s - jnp.concatenate([new] * (length // VD), axis=1))
                peaks[m, at, :] = new
                summed = totals[m, at, :] * factor
                for j in range(length // VD):
                    summed = summed + p[:, j * VD : (j + 1) * VD]
                totals[m, at, :] = summed
                weighted[m, at, :] = weighted[m, at, :] * factor + jnp.dot(
                    p.astype(bf16), value_block, preferred_element_type=f32
                )
            return carry

        lax.fori_loop(first, last, row_block, 0)

    def kv_pass(src, *ways):
        for array in (K, V):
            pass_on(array, src, *ways)

    per_block = length // rows
    spread_queries(q)
    attend(me, q * per_block, (q + 1) * per_block)
    kv_pass(mate, FAR, ACROSS)
    feed(GATE, ADJACENT, FAR, MATE, ACROSS)
    q_copy().wait_recv()
    spread_queries(1 - q)
    attend(me, (1 - q) * per_block, (2 - q) * per_block)
    attend(mate)
    kv_pass(across)
    attend(across)
    kv_pass(far, ACROSS)
    kv_pass(amate)
    attend(amate)
    kv_pass(fmate, ACROSS)
    pass_on(GATE, mate, FAR, ACROSS)
    feed(UP, ADJACENT, FAR, MATE, ACROSS)
    attend(far)
    ship(resid_copy(resid, t, {"sp": mate, "tp": 2 * x + q}, 2))
    attend(fmate)
    kv_pass(afar)
    attend(afar)
    feed(DOWN, ADJACENT, FAR, MATE)
    kv_pass(afmate)
    attend(afmate)

    head = 2 * t + q
    for b in range(2):
        at = slice(b * length, (b + 1) * length)
        first = weighted[0, at, :] / jnp.sum(totals[0, at, :], axis=1, keepdims=True)
        second = weighted[1, at, :] / jnp.sum(totals[1, at, :], axis=1, keepdims=True)
        mixed = first - mix_lambda[q] * second
        spread = jnp.mean(mixed * mixed, axis=1, keepdims=True)
        normed = mixed * lax.rsqrt(spread + 1e-06) * head_gain[...] * 0.8
        heads_own[b] = normed.astype(bf16)

        @pl.when(c == b)
        def _():
            heads_all[head] = heads_own[b]

    def head_copy(src, slot, target, send):
        return lambda: remote(
            src, heads_all.at[slot], head_send.at[send], head_recv.at[slot], target
        )

    for b in range(2):
        ship(head_copy(heads_own.at[b], head, {"sp": mate, "tp": 2 * x + b}, b))
    for b in range(2):
        ship(head_copy(heads_own.at[b], head, {"tp": 2 * (1 - x) + b}, 2 + b))
        ship(head_copy(heads_own.at[b], head, {"tp": sibling}, 4 + b), c != b)

    def head_wait(slot):
        head_copy(heads_all.at[slot], slot, {"tp": sibling}, 0)().wait_recv()

    out_copy(out_weight, xdev, sibling, 0)().wait_recv()
    ship(out_copy(out_all.at[xdev], xdev, sibling, 2))

    def resid_wait(slot):
        resid_copy(resid, slot, {"tp": sibling}, 0)().wait_recv()

    for k in range(2):
        slot = 2 * x + k
        when(c != q, lambda: resid_wait(slot))
        ship(resid_copy(resid_all.at[slot], slot, {"tp": xdev}, 3 + k), c != q)
    for k in range(2):
        slot = 2 * (2 * x + k) + 1 - q
        head_wait(slot)
        ship(head_copy(heads_all.at[slot], slot, {"tp": xdev}, 6 + k))

    pass_on(UP, mate, FAR, ACROSS)
    pass_on(GATE, far, ACROSS)
    fetched(early)

    out_copy(out_weight, sibling, sibling, 0)().wait_recv()
    out_copy(out_weight, xsib, sibling, 0)().wait_recv()
    for slot in (sibling, xdev, xsib):
        remote(
            norm_gain, gain_all.at[slot], gain_send.at[0], gain_recv.at[slot], {"tp": sibling}
        ).wait_recv()
    when(c == q, lambda: resid_wait(sibling))
    for k in range(2):
        resid_wait(2 * (1 - x) + k)
    head_wait(2 * sibling + q)
    for k in range(2):
        head_wait(2 * (2 * (1 - x) + k) + q)
    for k in range(2):
        head_wait(2 * (2 * (1 - x) + k) + 1 - q)

    row_sum = jnp.zeros((length, 1), f32)
    for j in range(tp):
        cols = slice(j * features, (j + 1) * features)
        total = resid_all[j].astype(f32) + jnp.dot(
            jnp.concatenate([heads_all[i] for i in range(heads_all.shape[0])], axis=1),
            out_all[j],
            preferred_element_type=f32,
        )
        after[:, cols] = total
        row_sum = row_sum + jnp.sum(total * total, axis=1, keepdims=True)
    inverse = lax.rsqrt(row_sum / D + 1e-06)
    for j in range(tp):
        cols = slice(j * features, (j + 1) * features)
        rows_all[c, EDGE : EDGE + length, cols] = (
            after[:, cols] * inverse * gain_all[j]
        ).astype(bf16)

    def row_copy(block):
        here = rows_all.at[block, pl.ds(EDGE, length)]
        return remote(here, here, row_sem.at[0], row_sem.at[1], {"tp": sibling})

    ship(lambda: row_copy(c))

    def own_features(device):
        return pl.ds(pl.multiple_of(device * features, features), features)

    def after_copy():
        return remote(
            after.at[:, own_features(sibling)],
            after_own,
            after_sem.at[0],
            after_sem.at[1],
            {"tp": sibling},
        )

    ship(after_copy, c == q)

    @pl.when(c == q)
    def _():
        after_own[...] = after[:, own_features(t)]

    pass_on(GATE, fmate, ACROSS)
    feed(DOWN, ACROSS)
    row_copy(1 - c).wait_recv()

    begin, end, top, bottom = EDGE, length, 0, EDGE + length

    def edge_copy(i, source_block, source, block, dest, target):
        def rows_at(start):
            return pl.ds(pl.multiple_of(start, EDGE), EDGE)

        return remote(
            rows_all.at[source_block, rows_at(source)],
            rows_all.at[block, rows_at(dest)],
            edge_send.at[i],
            edge_recv.at[i],
            {"sp": target},
        )

    def pick(first, second):
        return first + y * (second - first)

    def edge(i):
        return (
            lambda: edge_copy(0, 0, pick(end, begin), 0, pick(top, bottom), across),
            lambda: edge_copy(
                1, pick(1, 0), pick(begin, end), pick(0, 1), pick(bottom, top), across
            ),
            lambda: edge_copy(2, 1, pick(end, begin), 1, pick(top, bottom), across),
        )[i]

    for i in range(3):
        ship(edge(i))
    before = jnp.logical_and(y == 1, h == 0)
    behind = jnp.logical_and(y == 0, h == 1)
    onward = lambda: edge_copy(3, 1, end, 0, top, jnp.minimum(me + half_sp - 1, sp - 1))
    back = lambda: edge_copy(3, 0, begin, 1, bottom, jnp.maximum(me - half_sp + 1, 0))
    ship(onward, before)
    ship(back, behind)

    @pl.when(jnp.logical_and(y == 0, h == 0))
    def _():
        rows_all[0, 0:EDGE, :] = jnp.zeros((EDGE, rows_all.shape[2]), bf16)

    @pl.when(jnp.logical_and(y == 1, h == 1))
    def _():
        rows_all[1, EDGE + length :, :] = jnp.zeros((EDGE, rows_all.shape[2]), bf16)

    for array in (GATE, UP):
        arrive(array, across)
        arrive(array, amate)
    pass_on(DOWN, mate, FAR, ACROSS)

    for i in range(3):
        edge(i)().wait_recv()
    when(before, lambda: onward().wait_recv())
    when(behind, lambda: back().wait_recv())

    span = half_sp * depth
    wide = 2 * LANES

    def expand(acc, weight, half, start, count, fresh):
        deep = pl.ds(pl.multiple_of(half * span, span), span)
        blocks = pl.ds(half * half_sp, half_sp)

        def tile(i, carry):
            b, cols = rem(i, 2), pl.ds(pl.multiple_of(div(i, 2) * wide, wide), wide)
            part = jnp.dot(
                rows_all[b, start : start + count, deep],
                weight[blocks, :, cols].reshape(span, wide),
                preferred_element_type=f32,
            )
            if fresh:
                acc[b, :, cols] = part
            else:
                acc[b, :, cols] += part
            return carry

        lax.fori_loop(0, 2 * (big // wide), tile, 0)

    expand(gate_acc, gates, h, 0, length + 2 * EDGE, True)
    expand(up_acc, ups, h, EDGE, length, True)
    pass_on(UP, far, ACROSS)
    arrive(GATE, afar)
    arrive(GATE, afmate)
    expand(gate_acc, gates, 1 - h, 0, length + 2 * EDGE, False)
    pass_on(UP, fmate, ACROSS)
    arrive(UP, afar)
    arrive(UP, afmate)
    expand(up_acc, ups, 1 - h, EDGE, length, False)

    base = jnp.where(c == q, q * (ff - big), q * (ff - small))

    def activate(b, carry):
        for j in range(big // LANES):
            cols = slice(j * LANES, (j + 1) * LANES)
            spot = jnp.minimum(base + j * LANES, ff - LANES)
            taps = pl.ds(pl.multiple_of(spot, LANES), LANES)

            def fill():
                def tap(start):
                    return gate_acc[b, start : start + length, cols].astype(bf16).astype(f32)

                conv = (
                    tap(EDGE - 1) * conv_weight[0:1, taps]
                    + tap(EDGE) * conv_weight[1:2, taps]
                    + tap(EDGE + 1) * conv_weight[2:3, taps]
                    + conv_bias[:, taps]
                )
                hidden[b, :, cols] = (conv / (1.0 + jnp.exp(-conv)) * up_acc[b, :, cols]).astype(
                    bf16
                )

            if (j + 1) * LANES <= small:
                fill()
            else:
                pl.when(c == q)(fill)

                @pl.when(c != q)
                def _():
                    hidden[b, :, cols] = jnp.zeros((length, LANES), bf16)

        return carry

    lax.fori_loop(0, 2, activate, 0)

    per = sp // tp

    def owner(s):
        o = div(s, per)
        return div(o, 2), rem(o, 2)

    def core_slot(s):
        return div(s, half_sp) * per + rem(s, per)

    def core_copy(s):
        return remote(
            stage.at[s], from_core.at[core_slot(s)], part_send.at[s],
            core_recv.at[core_slot(s)], {"tp": sibling},
        )

    def x_copy(s):
        return remote(
            stage.at[s], from_x.at[rem(s, per)], part_send.at[s], x_recv.at[rem(s, per)],
            {"tp": xdev},
        )

    def z_copy(s):
        return remote(
            stage.at[s, 0], from_z.at[rem(s, per)], part_send.at[s], z_recv.at[rem(s, per)],
            {"sp": mate},
        )

    def multiply(s):
        ox, oc = owner(s)
        product = jnp.dot(
            hidden[...].reshape(2 * length, big), downs[s], preferred_element_type=f32
        ).reshape(2, length, down_cols)

        @pl.when(c != oc)
        def _():
            stage[s] = product.astype(bf16)

        @pl.when(c == oc)
        def _():
            held[core_slot(s)] = product

        ship(lambda: core_copy(s), c != oc)

    def add_core(s):
        ox, oc = owner(s)
        mine = c == oc
        slot = core_slot(s)
        when(mine, lambda: core_copy(s).wait_recv())

        @pl.when(jnp.logical_and(mine, x != ox))
        def _():
            stage[s] = (held[slot] + from_core[slot].astype(f32)).astype(bf16)

        ship(lambda: x_copy(s), jnp.logical_and(mine, x != ox))

    def out_cols(s):
        return pl.ds(pl.multiple_of(rem(s, per) * down_cols, down_cols), down_cols)

    def add_x(s):
        ox, oc = owner(s)
        mine = jnp.logical_and(c == oc, x == ox)
        slot = core_slot(s)

        def summed(b):
            return (
                held[slot, b]
                + from_core[slot, b].astype(f32)
                + from_x[rem(s, per), b].astype(f32)
            )

        @pl.when(mine)
        def _():
            x_copy(s).wait_recv()
            stage[s, 0] = summed(1 - q).astype(bf16)

        ship(lambda: z_copy(s), mine)

        @pl.when(mine)
        def _():
            after_own[:, out_cols(s)] += summed(q)

    near = (me, mate, across, amate)
    fetched_down = (across, amate)
    for s in fetched_down:
        arrive(DOWN, s)
    for s in near:
        multiply(s)
    for s in near:
        add_core(s)
    pass_on(DOWN, far, ACROSS)
    multiply(far)
    pass_on(DOWN, fmate, ACROSS)
    multiply(fmate)
    when(c != q, lambda: after_copy().wait_recv())
    for s in near:
        add_x(s)
    add_core(far)
    add_core(fmate)
    for s in (afar, afmate):
        arrive(DOWN, s)
        multiply(s)
    for s in (afar, afmate):
        add_core(s)
    for s in (far, fmate, afar, afmate):
        add_x(s)
    for k in range(per):
        cols = slice(k * down_cols, (k + 1) * down_cols)
        z_copy(k).wait_recv()
        out[:, cols] = (after_own[:, cols] + from_z[k].astype(f32)).astype(bf16)

    for cond, make in drains:
        when(cond, lambda: make().wait_send())


def fused(sp, tp, *args):
    resid, queries, keys, values = args[:4]
    gate_weight, down_weight = args[8], args[12]
    length, width = queries.shape
    features = resid.shape[1]
    depth, ff = gate_weight.shape
    maps = 2
    heads = tp * (width // VD)
    full = tp * features
    bf16, f32 = jnp.bfloat16, jnp.float32
    dma = pltpu.SemaphoreType.DMA
    vmem = pl.BlockSpec(memory_space=pltpu.VMEM)
    smem = pl.BlockSpec(memory_space=pltpu.SMEM)
    hbm = pl.BlockSpec(memory_space=pl.ANY)
    rows = length + 2 * EDGE
    down_cols = down_weight.shape[1]
    tiles = ff // LANES
    big = (tiles - tiles // 2) * LANES
    per = sp // tp
    args = list(args)
    for i in (5, 7, 11):
        args[i] = args[i].reshape(1, -1)
    return pl.pallas_call(
        functools.partial(layer_kernel, sp, tp),
        out_shape=jax.ShapeDtypeStruct(resid.shape, bf16),
        in_specs=[
            hbm, hbm, hbm, hbm, smem, vmem, hbm, vmem, hbm, hbm, vmem, vmem, hbm,
        ],
        out_specs=vmem,
        scratch_shapes=[
            pltpu.VMEM((2, length, VD), bf16),
            pltpu.VMEM((maps, 2 * length, VD), bf16),
            pltpu.VMEM((sp, 2, length, VD), bf16),
            pltpu.VMEM((sp, depth, big), bf16),
            pltpu.VMEM((sp, depth, big), bf16),
            pltpu.VMEM((sp, big, down_cols), bf16),
            pltpu.VMEM((maps, 2 * length, LANES), f32),
            pltpu.VMEM((maps, 2 * length, LANES), f32),
            pltpu.VMEM((maps, 2 * length, VD), f32),
            pltpu.VMEM((2, length, VD), bf16),
            pltpu.VMEM((heads, length, VD), bf16),
            pltpu.VMEM((tp, heads * VD, features), bf16),
            pltpu.VMEM((tp, length, features), bf16),
            pltpu.VMEM((tp, 1, features), f32),
            pltpu.VMEM((length, full), f32),
            pltpu.VMEM((length, features), f32),
            pltpu.VMEM((2, rows, full), bf16),
            pltpu.VMEM((2, rows, big), f32),
            pltpu.VMEM((2, length, big), f32),
            pltpu.VMEM((2, length, big), bf16),
            pltpu.VMEM((2 * per, 2, length, down_cols), f32),
            pltpu.VMEM((sp, 2, length, down_cols), bf16),
            pltpu.VMEM((2 * per, 2, length, down_cols), bf16),
            pltpu.VMEM((per, 2, length, down_cols), bf16),
            pltpu.VMEM((per, length, down_cols), bf16),
            dma((12,)),
            dma((5, 4, sp)),
            dma((5, sp)),
            dma((2,)),
            dma((8,)),
            dma((heads,)),
            dma((3,)),
            dma((tp,)),
            dma((5,)),
            dma((tp,)),
            dma((3,)),
            dma((tp,)),
            dma((2,)),
            dma((2,)),
            dma((4,)),
            dma((4,)),
            dma((sp,)),
            dma((2 * per,)),
            dma((per,)),
            dma((per,)),
        ],
        compiler_params=pltpu.CompilerParams(
            has_side_effects=True, vmem_limit_bytes=60 * 1024 * 1024
        ),
    )(*args)


def solution(mesh):
    sp, tp = mesh.shape["sp"], mesh.shape["tp"]

    def run(*args):
        width, (depth, ff) = args[1].shape[1], args[8].shape
        small = args[0].shape[0] <= 512
        pairs = tp == 4 and sp == 2 * tp
        if pairs and small and depth % 256 == 0 and width == 2 * VD and ff % 256 == 128:
            return fused(sp, tp, *args)
        return on_device(*args)

    placed = (
        P("sp", "tp"),
        P("sp", "tp"),
        P("sp", "tp"),
        P("sp", "tp"),
        P("tp"),
        P(),
        P(None, "tp"),
        P("tp"),
        P("sp", "tp"),
        P("sp", "tp"),
        P(None, "tp"),
        P("tp"),
        P("tp", "sp"),
    )
    return jax.shard_map(
        run, mesh=mesh, in_specs=placed, out_specs=P("sp", "tp"), check_vma=False
    )
```

time: 305 us -> 229 us (0.75)
  the two profiles are of different devices: /device:TPU:0 before, /device:TPU:16 now
where the time goes in v1:
time: 229 us
  Pallas kernels  226 us (99%)
  local copies, waits for them, and re-layouts  3.16 us (1%)
    pallas_call x1, Pallas kernels, fused(): pl.pallas_call(functools.partial(layer_kernel, sp, tp), out_shape=jax.Sha...  226 us

profile of v1, /device:TPU:16, one launch (start us, length us, event | category | flops | bytes accessed | tf_op | source)
XLA Modules:
  0.0 228.9 jit_solution(2045341949618543778)
XLA Ops:
  0.0 1.3 reshape.11.conv_bias
  1.3 225.7 %shard_map.127 = bf16[512,512]{1,0:T(8,128)(2,1)} custom-call(bf16[512,512]{1,0:T(8,128)(2,1)} %resid.1, bf16[512,256]{1,0:T(8,128)(2,1)} %queries.1, bf16[512,256]{1,0:T(8,128)(2,1)} %keys.1, bf16[512,256]{1,0:T(8,128)(2,1)} %values.1, f32[2]{0:T(128)} %mix_lambda.1, f32[1,128]{1,0:T(1,128)} %bitcast.3, bf16[1024,512]{1,0:T(8,128)(2,1)} %out_weight.1, ...), custom_call_target="tpu_custom_call" | custom-call | tf_op jit(solution)/shard_map/pallas_call | solution.py:817
  227.0 1.9 copy.15

commit v2 on v1

--- a/solution.py
+++ b/solution.py
@@ -212,7 +212,7 @@
     amate = across + 2 - 4 * q
     afar = across + 4 - 8 * h
     afmate = afar + 2 - 4 * q
-    inner = h != q
+    inner, outer = h != q, h == q
     sibling = t + 1 - 2 * c
     xdev = t + 2 - 4 * x
     xsib = sibling + 2 - 4 * x
@@ -288,13 +288,13 @@
 
             ship(make, both(cond, which) if which is not None else cond)
 
-    def feed(array, *ways):
+    def feed(array, *ways, cond=None):
         other = 1 - q
         for way in ways:
             if way == ACROSS:
                 send(array, me, ACROSS, across, part=q)
             elif way == FAR:
-                send(array, me, FAR, far, part=q)
+                send(array, me, FAR, far, part=q, cond=cond)
             elif way == MATE:
                 send(array, me, MATE, mate, part=other)
             else:
@@ -321,7 +321,7 @@
 
     for way in (MATE, ADJACENT, FAR, ACROSS):
         for array in (K, V):
-            feed(array, way)
+            feed(array, way, cond=inner)
 
     def q_copy():
         cols = pl.ds(pl.multiple_of((1 - q) * VD, VD), VD)
@@ -427,8 +427,12 @@
     per_block = length // rows
     spread_queries(q)
     attend(me, q * per_block, (q + 1) * per_block)
+    for array in (K, V):
+        feed(array, FAR, cond=outer)
+    ship(resid_copy(resid, t, {"sp": mate, "tp": 2 * x + q}, 2))
+    feed(GATE, ACROSS)
     kv_pass(mate, FAR, ACROSS)
-    feed(GATE, ADJACENT, FAR, MATE, ACROSS)
+    feed(GATE, ADJACENT, FAR, MATE)
     q_copy().wait_recv()
     spread_queries(1 - q)
     attend(me, (1 - q) * per_block, (2 - q) * per_block)
@@ -439,14 +443,24 @@
     kv_pass(amate)
     attend(amate)
     kv_pass(fmate, ACROSS)
-    pass_on(GATE, mate, FAR, ACROSS)
-    feed(UP, ADJACENT, FAR, MATE, ACROSS)
+    feed(UP, ACROSS)
     attend(far)
-    ship(resid_copy(resid, t, {"sp": mate, "tp": 2 * x + q}, 2))
+
+    def resid_wait(slot):
+        resid_copy(resid, slot, {"tp": sibling}, 0)().wait_recv()
+
+    for k in range(2):
+        slot = 2 * x + k
+        when(c != q, lambda: resid_wait(slot))
+        ship(resid_copy(resid_all.at[slot], slot, {"tp": xdev}, 3 + k), c != q)
+    out_copy(out_weight, xdev, sibling, 0)().wait_recv()
+    ship(out_copy(out_all.at[xdev], xdev, sibling, 2))
     attend(fmate)
     kv_pass(afar)
     attend(afar)
-    feed(DOWN, ADJACENT, FAR, MATE)
+    pass_on(GATE, mate, FAR, ACROSS)
+    feed(UP, ADJACENT)
+    feed(UP, FAR, cond=inner)
     kv_pass(afmate)
     attend(afmate)
 
@@ -475,26 +489,18 @@
         ship(head_copy(heads_own.at[b], head, {"tp": 2 * (1 - x) + b}, 2 + b))
         ship(head_copy(heads_own.at[b], head, {"tp": sibling}, 4 + b), c != b)
 
+    feed(UP, MATE)
+    feed(UP, FAR, cond=outer)
+
     def head_wait(slot):
         head_copy(heads_all.at[slot], slot, {"tp": sibling}, 0)().wait_recv()
 
-    out_copy(out_weight, xdev, sibling, 0)().wait_recv()
-    ship(out_copy(out_all.at[xdev], xdev, sibling, 2))
-
-    def resid_wait(slot):
-        resid_copy(resid, slot, {"tp": sibling}, 0)().wait_recv()
-
-    for k in range(2):
-        slot = 2 * x + k
-        when(c != q, lambda: resid_wait(slot))
-        ship(resid_copy(resid_all.at[slot], slot, {"tp": xdev}, 3 + k), c != q)
+    pass_on(GATE, far, ACROSS)
     for k in range(2):
         slot = 2 * (2 * x + k) + 1 - q
         head_wait(slot)
         ship(head_copy(heads_all.at[slot], slot, {"tp": xdev}, 6 + k))
 
-    pass_on(UP, mate, FAR, ACROSS)
-    pass_on(GATE, far, ACROSS)
     fetched(early)
 
     out_copy(out_weight, sibling, sibling, 0)().wait_recv()
@@ -554,7 +560,8 @@
         after_own[...] = after[:, own_features(t)]
 
     pass_on(GATE, fmate, ACROSS)
-    feed(DOWN, ACROSS)
+    pass_on(UP, mate, FAR, ACROSS)
+    feed(DOWN, ADJACENT, FAR, MATE)
     row_copy(1 - c).wait_recv()
 
     begin, end, top, bottom = EDGE, length, 0, EDGE + length
@@ -600,48 +607,66 @@
     def _():
         rows_all[1, EDGE + length :, :] = jnp.zeros((EDGE, rows_all.shape[2]), bf16)
 
-    for array in (GATE, UP):
-        arrive(array, across)
-        arrive(array, amate)
-    pass_on(DOWN, mate, FAR, ACROSS)
-
+    arrive(GATE, across)
+    arrive(GATE, amate)
+
+    span = half_sp * depth
+    wide = 2 * LANES
+
+    def expand(acc, weight, half, fresh):
+        offset = EDGE if acc is gate_acc else 0
+        held_rows = pl.ds(offset, length)
+        deep = pl.ds(pl.multiple_of(half * span, span), span)
+        blocks = pl.ds(half * half_sp, half_sp)
+
+        def tile(i, carry):
+            b, cols = rem(i, 2), pl.ds(pl.multiple_of(div(i, 2) * wide, wide), wide)
+            part = jnp.dot(
+                rows_all[b, EDGE : EDGE + length, deep],
+                weight[blocks, :, cols].reshape(span, wide),
+                preferred_element_type=f32,
+            )
+            if fresh:
+                acc[b, held_rows, cols] = part
+            else:
+                acc[b, held_rows, cols] += part
+            return carry
+
+        lax.fori_loop(0, 2 * (big // wide), tile, 0)
+
+    expand(gate_acc, gates, h, True)
+    arrive(GATE, afar)
+    arrive(GATE, afmate)
+    expand(gate_acc, gates, 1 - h, False)
+    pass_on(UP, far, ACROSS)
+    arrive(UP, across)
+    arrive(UP, amate)
+    expand(up_acc, ups, h, True)
+    pass_on(DOWN, mate, FAR)
+    pass_on(UP, fmate, ACROSS)
+    feed(DOWN, ACROSS)
+    send(DOWN, mate, ACROSS, across)
     for i in range(3):
         edge(i)().wait_recv()
     when(before, lambda: onward().wait_recv())
     when(behind, lambda: back().wait_recv())
 
-    span = half_sp * depth
-    wide = 2 * LANES
-
-    def expand(acc, weight, half, start, count, fresh):
-        deep = pl.ds(pl.multiple_of(half * span, span), span)
-        blocks = pl.ds(half * half_sp, half_sp)
-
-        def tile(i, carry):
-            b, cols = rem(i, 2), pl.ds(pl.multiple_of(div(i, 2) * wide, wide), wide)
-            part = jnp.dot(
-                rows_all[b, start : start + count, deep],
-                weight[blocks, :, cols].reshape(span, wide),
-                preferred_element_type=f32,
-            )
-            if fresh:
-                acc[b, :, cols] = part
-            else:
-                acc[b, :, cols] += part
-            return carry
-
-        lax.fori_loop(0, 2 * (big // wide), tile, 0)
-
-    expand(gate_acc, gates, h, 0, length + 2 * EDGE, True)
-    expand(up_acc, ups, h, EDGE, length, True)
-    pass_on(UP, far, ACROSS)
-    arrive(GATE, afar)
-    arrive(GATE, afmate)
-    expand(gate_acc, gates, 1 - h, 0, length + 2 * EDGE, False)
-    pass_on(UP, fmate, ACROSS)
+    def halo(i, carry):
+        cols = pl.ds(pl.multiple_of(i * wide, wide), wide)
+        sides = (slice(0, EDGE), slice(EDGE + length, length + 2 * EDGE))
+        part = jnp.dot(
+            jnp.concatenate([rows_all[b, side, :] for b in range(2) for side in sides], axis=0),
+            gates[:, :, cols].reshape(sp * depth, wide),
+            preferred_element_type=f32,
+        )
+        for k in range(4):
+            gate_acc[k // 2, sides[k % 2], cols] = part[k * EDGE : (k + 1) * EDGE]
+        return carry
+
+    lax.fori_loop(0, big // wide, halo, 0)
     arrive(UP, afar)
     arrive(UP, afmate)
-    expand(up_acc, ups, 1 - h, EDGE, length, False)
+    expand(up_acc, ups, 1 - h, False)
 
     base = jnp.where(c == q, q * (ff - big), q * (ff - small))
 
@@ -689,20 +714,20 @@
 
     def core_copy(s):
         return remote(
-            stage.at[s], from_core.at[core_slot(s)], part_send.at[s],
+            stage.at[s], from_core.at[core_slot(s)], part_send.at[0, s],
             core_recv.at[core_slot(s)], {"tp": sibling},
+        )
+
+    def z_copy(s):
+        return remote(
+            stage.at[s, 0], from_z.at[core_slot(s)], part_send.at[0, s],
+            z_recv.at[core_slot(s)], {"sp": mate},
         )
 
     def x_copy(s):
         return remote(
-            stage.at[s], from_x.at[rem(s, per)], part_send.at[s], x_recv.at[rem(s, per)],
+            stage.at[s, 1], from_x.at[rem(s, per)], part_send.at[1, s], x_recv.at[rem(s, per)],
             {"tp": xdev},
-        )
-
-    def z_copy(s):
-        return remote(
-            stage.at[s, 0], from_z.at[rem(s, per)], part_send.at[s], z_recv.at[rem(s, per)],
-            {"sp": mate},
         )
 
     def multiply(s):
@@ -725,68 +750,72 @@
         ox, oc = owner(s)
         mine = c == oc
         slot = core_slot(s)
-        when(mine, lambda: core_copy(s).wait_recv())
+
+        @pl.when(mine)
+        def _():
+            core_copy(s).wait_recv()
+            stage[s, 0] = (held[slot, 1 - q] + from_core[slot, 1 - q].astype(f32)).astype(bf16)
+
+        ship(lambda: z_copy(s), mine)
+
+    def out_cols(s):
+        return pl.ds(pl.multiple_of(rem(s, per) * down_cols, down_cols), down_cols)
+
+    def add_z(s):
+        ox, oc = owner(s)
+        mine = c == oc
+        slot = core_slot(s)
+
+        def summed():
+            return (
+                held[slot, q] + from_core[slot, q].astype(f32) + from_z[slot].astype(f32)
+            )
+
+        when(mine, lambda: z_copy(s).wait_recv())
+
+        @pl.when(jnp.logical_and(mine, x == ox))
+        def _():
+            after_own[:, out_cols(s)] += summed()
 
         @pl.when(jnp.logical_and(mine, x != ox))
         def _():
-            stage[s] = (held[slot] + from_core[slot].astype(f32)).astype(bf16)
+            stage[s, 1] = summed().astype(bf16)
 
         ship(lambda: x_copy(s), jnp.logical_and(mine, x != ox))
 
-    def out_cols(s):
-        return pl.ds(pl.multiple_of(rem(s, per) * down_cols, down_cols), down_cols)
-
-    def add_x(s):
-        ox, oc = owner(s)
-        mine = jnp.logical_and(c == oc, x == ox)
-        slot = core_slot(s)
-
-        def summed(b):
-            return (
-                held[slot, b]
-                + from_core[slot, b].astype(f32)
-                + from_x[rem(s, per), b].astype(f32)
-            )
-
-        @pl.when(mine)
-        def _():
-            x_copy(s).wait_recv()
-            stage[s, 0] = summed(1 - q).astype(bf16)
-
-        ship(lambda: z_copy(s), mine)
-
-        @pl.when(mine)
-        def _():
-            after_own[:, out_cols(s)] += summed(q)
-
-    near = (me, mate, across, amate)
-    fetched_down = (across, amate)
-    for s in fetched_down:
-        arrive(DOWN, s)
-    for s in near:
-        multiply(s)
-    for s in near:
-        add_core(s)
+    multiply(me)
+    multiply(mate)
+    add_core(me)
     pass_on(DOWN, far, ACROSS)
+    arrive(DOWN, across)
+    multiply(across)
+    add_core(mate)
+    arrive(DOWN, amate)
+    multiply(amate)
+    add_core(across)
+    pass_on(DOWN, fmate, ACROSS)
     multiply(far)
-    pass_on(DOWN, fmate, ACROSS)
+    add_core(amate)
     multiply(fmate)
+    add_core(far)
     when(c != q, lambda: after_copy().wait_recv())
-    for s in near:
-        add_x(s)
-    add_core(far)
+    add_z(me)
+    add_z(mate)
+    arrive(DOWN, afar)
+    multiply(afar)
     add_core(fmate)
-    for s in (afar, afmate):
-        arrive(DOWN, s)
-        multiply(s)
-    for s in (afar, afmate):
-        add_core(s)
+    add_z(across)
+    add_z(amate)
+    arrive(DOWN, afmate)
+    multiply(afmate)
+    add_core(afar)
+    add_core(afmate)
     for s in (far, fmate, afar, afmate):
-        add_x(s)
+        add_z(s)
     for k in range(per):
         cols = slice(k * down_cols, (k + 1) * down_cols)
-        z_copy(k).wait_recv()
-        out[:, cols] = (after_own[:, cols] + from_z[k].astype(f32)).astype(bf16)
+        x_copy(k).wait_recv()
+        out[:, cols] = (after_own[:, cols] + from_x[k].astype(f32)).astype(bf16)
 
     for cond, make in drains:
         when(cond, lambda: make().wait_send())
@@ -845,8 +874,8 @@
             pltpu.VMEM((2 * per, 2, length, down_cols), f32),
             pltpu.VMEM((sp, 2, length, down_cols), bf16),
             pltpu.VMEM((2 * per, 2, length, down_cols), bf16),
-            pltpu.VMEM((per, 2, length, down_cols), bf16),
             pltpu.VMEM((per, length, down_cols), bf16),
+            pltpu.VMEM((2 * per, length, down_cols), bf16),
             dma((12,)),
             dma((5, 4, sp)),
             dma((5, sp)),
@@ -863,10 +892,10 @@
             dma((2,)),
             dma((4,)),
             dma((4,)),
-            dma((sp,)),
+            dma((2, sp)),
             dma((2 * per,)),
             dma((per,)),
-            dma((per,)),
+            dma((2 * per,)),
         ],
         compiler_params=pltpu.CompilerParams(
             has_side_effects=True, vmem_limit_bytes=60 * 1024 * 1024

time: 229 us -> 175 us (0.76)
  the two profiles are of different devices: /device:TPU:16 before, /device:TPU:0 now
where the time goes in v2:
time: 175 us; the launch traced here: 171 us
  Pallas kernels  168 us (96%)
  local copies, waits for them, and re-layouts  3.16 us (2%)
    pallas_call x1, Pallas kernels, fused(): pl.pallas_call(functools.partial(layer_kernel, sp, tp), out_shape=jax.Sha...  168 us

profile of v2, /device:TPU:0, one launch (start us, length us, event | category | flops | bytes accessed | tf_op | source)
XLA Modules:
  0.0 171.1 jit_solution(371291290079938506)
XLA Ops:
  0.0 1.3 reshape.11.conv_bias
  1.3 168.0 %shard_map.127 = bf16[512,512]{1,0:T(8,128)(2,1)} custom-call(bf16[512,512]{1,0:T(8,128)(2,1)} %resid.1, bf16[512,256]{1,0:T(8,128)(2,1)} %queries.1, bf16[512,256]{1,0:T(8,128)(2,1)} %keys.1, bf16[512,256]{1,0:T(8,128)(2,1)} %values.1, f32[2]{0:T(128)} %mix_lambda.1, f32[1,128]{1,0:T(1,128)} %bitcast.3, bf16[1024,512]{1,0:T(8,128)(2,1)} %out_weight.1, ...), custom_call_target="tpu_custom_call" | custom-call | tf_op jit(solution)/shard_map/pallas_call | solution.py:846
  169.3 1.9 %copy.15 = bf16[512,512]{1,0:T(8,128)(2,1)} copy(bf16[512,512]{1,0:T(8,128)(2,1)} %shard_map.127) | data formatting | bytes 1048576

commit v3 on v2

--- a/solution.py
+++ b/solution.py
@@ -296,11 +296,11 @@
             elif way == FAR:
                 send(array, me, FAR, far, part=q, cond=cond)
             elif way == MATE:
-                send(array, me, MATE, mate, part=other)
+                send(array, me, MATE, mate, part=other, cond=cond)
             else:
                 send(array, me, ADJACENT, adjacent, part=other, cond=inner)
 
-    def arrive(array, src):
+    def arrive(array, src, cond=None):
         for which, size in variants(array, q):
 
             def wait(size=size):
@@ -309,25 +309,55 @@
                     here, here, send_sem.at[array, 0, src], recv_sem.at[array, src], {"sp": across}
                 ).wait_recv()
 
-            when(which, wait)
-
-    def pass_on(array, src, *ways):
-        arrive(array, src)
+            when(both(cond, which) if which is not None else cond, wait)
+
+    def pass_on(array, src, *ways, cond=None):
+        arrive(array, src, cond)
         for way in ways:
             if way == FAR:
                 send(array, src, FAR, far, cond=inner)
             else:
-                send(array, src, ACROSS, across)
-
-    for way in (MATE, ADJACENT, FAR, ACROSS):
+                send(array, src, ACROSS, across, cond=cond)
+
+    before = jnp.logical_and(y == 1, h == 0)
+    behind = jnp.logical_and(y == 0, h == 1)
+    later = jnp.minimum(me + half_sp - 1, sp - 1)
+    earlier = jnp.maximum(me - half_sp + 1, 0)
+    barrier = pltpu.get_barrier_semaphore()
+
+    def greet(target, cond=None):
+        when(
+            cond,
+            lambda: pl.semaphore_signal(
+                barrier, inc=1, device_id=target, device_id_type=pl.DeviceIdType.MESH
+            ),
+        )
+
+    for target in (
+        {"sp": far},
+        {"sp": mate},
+        {"sp": mate, "tp": sibling},
+        {"sp": across},
+        {"tp": xdev},
+        {"tp": xsib},
+        {"tp": sibling},
+    ):
+        greet(target)
+    greet({"sp": adjacent}, inner)
+    greet({"sp": later}, before)
+    greet({"sp": earlier}, behind)
+    pl.semaphore_wait(
+        barrier,
+        7 + jnp.where(inner, 1, 0) + jnp.where(jnp.logical_or(before, behind), 1, 0),
+    )
+
+    for way in (MATE, ADJACENT, ACROSS):
         for array in (K, V):
-            feed(array, way, cond=inner)
+            feed(array, way)
 
     def q_copy():
         cols = pl.ds(pl.multiple_of((1 - q) * VD, VD), VD)
         return remote(queries.at[:, cols], q_all.at[q], q_sem.at[0], q_sem.at[1], {"sp": mate})
-
-    ship(q_copy)
 
     local = []
 
@@ -428,22 +458,25 @@
     spread_queries(q)
     attend(me, q * per_block, (q + 1) * per_block)
     for array in (K, V):
-        feed(array, FAR, cond=outer)
+        feed(array, FAR)
+    ship(q_copy)
     ship(resid_copy(resid, t, {"sp": mate, "tp": 2 * x + q}, 2))
     feed(GATE, ACROSS)
     kv_pass(mate, FAR, ACROSS)
     feed(GATE, ADJACENT, FAR, MATE)
+    attend(mate, q * per_block, (q + 1) * per_block)
+    kv_pass(across)
+    attend(across, q * per_block, (q + 1) * per_block)
     q_copy().wait_recv()
     spread_queries(1 - q)
-    attend(me, (1 - q) * per_block, (2 - q) * per_block)
-    attend(mate)
-    kv_pass(across)
-    attend(across)
+    for src in (me, mate, across):
+        attend(src, (1 - q) * per_block, (2 - q) * per_block)
     kv_pass(far, ACROSS)
     kv_pass(amate)
     attend(amate)
     kv_pass(fmate, ACROSS)
     feed(UP, ACROSS)
+    feed(DOWN, ACROSS)
     attend(far)
 
     def resid_wait(slot):
@@ -458,7 +491,7 @@
     attend(fmate)
     kv_pass(afar)
     attend(afar)
-    pass_on(GATE, mate, FAR, ACROSS)
+    pass_on(GATE, mate, FAR, ACROSS, cond=inner)
     feed(UP, ADJACENT)
     feed(UP, FAR, cond=inner)
     kv_pass(afmate)
@@ -495,7 +528,9 @@
     def head_wait(slot):
         head_copy(heads_all.at[slot], slot, {"tp": sibling}, 0)().wait_recv()
 
-    pass_on(GATE, far, ACROSS)
+    pass_on(GATE, far, ACROSS, cond=inner)
+    pass_on(GATE, mate, ACROSS, cond=outer)
+    pass_on(GATE, far, ACROSS, cond=outer)
     for k in range(2):
         slot = 2 * (2 * x + k) + 1 - q
         head_wait(slot)
@@ -518,6 +553,7 @@
     for k in range(2):
         head_wait(2 * (2 * (1 - x) + k) + 1 - q)
 
+    pass_on(GATE, fmate, ACROSS)
     row_sum = jnp.zeros((length, 1), f32)
     for j in range(tp):
         cols = slice(j * features, (j + 1) * features)
@@ -559,9 +595,7 @@
     def _():
         after_own[...] = after[:, own_features(t)]
 
-    pass_on(GATE, fmate, ACROSS)
-    pass_on(UP, mate, FAR, ACROSS)
-    feed(DOWN, ADJACENT, FAR, MATE)
+    pass_on(UP, mate, FAR, ACROSS, cond=inner)
     row_copy(1 - c).wait_recv()
 
     begin, end, top, bottom = EDGE, length, 0, EDGE + length
@@ -592,12 +626,11 @@
 
     for i in range(3):
         ship(edge(i))
-    before = jnp.logical_and(y == 1, h == 0)
-    behind = jnp.logical_and(y == 0, h == 1)
-    onward = lambda: edge_copy(3, 1, end, 0, top, jnp.minimum(me + half_sp - 1, sp - 1))
-    back = lambda: edge_copy(3, 0, begin, 1, bottom, jnp.maximum(me - half_sp + 1, 0))
+    onward = lambda: edge_copy(3, 1, end, 0, top, later)
+    back = lambda: edge_copy(3, 0, begin, 1, bottom, earlier)
     ship(onward, before)
     ship(back, behind)
+    feed(DOWN, ADJACENT, FAR, MATE)
 
     @pl.when(jnp.logical_and(y == 0, h == 0))
     def _():
@@ -635,16 +668,16 @@
         lax.fori_loop(0, 2 * (big // wide), tile, 0)
 
     expand(gate_acc, gates, h, True)
+    pass_on(UP, mate, ACROSS, cond=outer)
     arrive(GATE, afar)
     arrive(GATE, afmate)
     expand(gate_acc, gates, 1 - h, False)
+    arrive(UP, across)
     pass_on(UP, far, ACROSS)
-    arrive(UP, across)
+    pass_on(UP, fmate, ACROSS)
     arrive(UP, amate)
     expand(up_acc, ups, h, True)
     pass_on(DOWN, mate, FAR)
-    pass_on(UP, fmate, ACROSS)
-    feed(DOWN, ACROSS)
     send(DOWN, mate, ACROSS, across)
     for i in range(3):
         edge(i)().wait_recv()
@@ -684,7 +717,7 @@
                     tap(EDGE - 1) * conv_weight[0:1, taps]
                     + tap(EDGE) * conv_weight[1:2, taps]
                     + tap(EDGE + 1) * conv_weight[2:3, taps]
-                    + conv_bias[:, taps]
+                    + conv_bias[pl.ds(div(spot, LANES), 1), :]
                 )
                 hidden[b, :, cols] = (conv / (1.0 + jnp.exp(-conv)) * up_acc[b, :, cols]).astype(
                     bf16
@@ -841,8 +874,9 @@
     big = (tiles - tiles // 2) * LANES
     per = sp // tp
     args = list(args)
-    for i in (5, 7, 11):
+    for i in (5, 7):
         args[i] = args[i].reshape(1, -1)
+    args[11] = args[11].reshape(-1, LANES)
     return pl.pallas_call(
         functools.partial(layer_kernel, sp, tp),
         out_shape=jax.ShapeDtypeStruct(resid.shape, bf16),
@@ -898,7 +932,7 @@
             dma((2 * per,)),
         ],
         compiler_params=pltpu.CompilerParams(
-            has_side_effects=True, vmem_limit_bytes=60 * 1024 * 1024
+            has_side_effects=True, collective_id=0, vmem_limit_bytes=60 * 1024 * 1024
         ),
     )(*args)
 

time: 175 us -> 160 us (0.914); the launches traced: 171 us -> 160 us
  Pallas kernels: 168 us -> 158 us
    pallas_call x1, Pallas kernels: 168 us -> 158 us  [fused(): pl.pallas_call(functools.partial(layer_kernel, sp, tp), out_shape=jax.Sha...]
where the time goes in v3:
time: 160 us
  Pallas kernels  158 us (99%)
  local copies, waits for them, and re-layouts  1.87 us (1%)
    pallas_call x1, Pallas kernels, fused(): pl.pallas_call(functools.partial(layer_kernel, sp, tp), out_shape=jax.Sha...  158 us

profile of v3, /device:TPU:0, one launch (start us, length us, event | category | flops | bytes accessed | tf_op | source)
XLA Modules:
  0.0 159.7 jit_solution(12428652905955088354)
XLA Ops:
  0.0 157.8 %shard_map.127 = bf16[512,512]{1,0:T(8,128)(2,1)} custom-call(bf16[512,512]{1,0:T(8,128)(2,1)} %resid.1, bf16[512,256]{1,0:T(8,128)(2,1)} %queries.1, bf16[512,256]{1,0:T(8,128)(2,1)} %keys.1, bf16[512,256]{1,0:T(8,128)(2,1)} %values.1, f32[2]{0:T(128)} %mix_lambda.1, f32[1,128]{1,0:T(1,128)} %bitcast.5, bf16[1024,512]{1,0:T(8,128)(2,1)} %out_weight.1, ...), custom_call_target="tpu_custom_call" | custom-call | tf_op jit(solution)/shard_map/pallas_call | solution.py:880
  157.8 1.9 %copy.15 = bf16[512,512]{1,0:T(8,128)(2,1)} copy(bf16[512,512]{1,0:T(8,128)(2,1)} %shard_map.127) | data formatting | bytes 1048576

commit v4 on v3

--- a/solution.py
+++ b/solution.py
@@ -170,12 +170,14 @@
     rows_all,
     gate_acc,
     up_acc,
+    active,
     hidden,
     held,
     stage,
     from_core,
     from_x,
     from_z,
+    done,
     local_sem,
     send_sem,
     recv_sem,
@@ -224,7 +226,8 @@
     small = ff - big
     down_cols = down_weight.shape[1]
     half_sp = sp // 2
-    K, V, GATE, UP, DOWN = range(5)
+    K, V = 0, 1
+    KEYS, GATE, UP, DOWN = (K, V), (2,), (3, 4), (5, 6)
     ACROSS, FAR, MATE, ADJACENT = range(4)
 
     drains = []
@@ -253,25 +256,40 @@
         drains.append((cond, make))
 
     def variants(array, part):
-        if array in (K, V):
+        if array in KEYS:
             return ((None, 0),)
         return ((c == part, big), (c != part, small))
 
     def landing(array, src, size):
-        if array in (K, V):
+        if array in KEYS:
             return kv.at[src, array]
-        if array == DOWN:
-            return downs.at[src, pl.ds(0, size)]
-        return (gates, ups)[array - GATE].at[src, :, pl.ds(0, size)]
+        if array in DOWN:
+            rows = size // len(DOWN)
+            return downs.at[src, pl.ds((array - DOWN[0]) * rows, rows)]
+        if array in UP:
+            rows = depth // len(UP)
+            return ups.at[src, pl.ds((array - UP[0]) * rows, rows), pl.ds(0, size)]
+        return gates.at[src, :, pl.ds(0, size)]
 
     def origin(array, part, size):
-        if array in (K, V):
+        if array in KEYS:
             cols = pl.ds(pl.multiple_of(part * VD, VD), VD)
             return (keys, values)[array].at[:, cols]
-        cut = pl.ds(pl.multiple_of(part * (ff - size), LANES), size)
-        if array == DOWN:
-            return down_weight.at[cut]
-        return (gate_weight, up_weight)[array - GATE].at[:, cut]
+        start = part * (ff - size)
+        if array in DOWN:
+            rows = size // len(DOWN)
+            first = start + (array - DOWN[0]) * rows
+            return down_weight.at[pl.ds(pl.multiple_of(first, LANES // 2), rows)]
+        cut = pl.ds(pl.multiple_of(start, LANES), size)
+        if array in UP:
+            rows = depth // len(UP)
+            return up_weight.at[pl.ds((array - UP[0]) * rows, rows), cut]
+        return gate_weight.at[:, cut]
+
+    def send_slot(way, src):
+        if src is me:
+            return way
+        return 4 if way == FAR else {id(mate): 5, id(far): 6, id(fmate): 7}[id(src)]
 
     def send(array, src, way, target, part=None, cond=None):
         for which, size in variants(array, q if part is None else part):
@@ -281,43 +299,46 @@
                 return remote(
                     here if part is None else origin(array, part, size),
                     here,
-                    send_sem.at[array, way, src],
+                    send_sem.at[array, send_slot(way, src)],
                     recv_sem.at[array, src],
                     {"sp": target},
                 )
 
             ship(make, both(cond, which) if which is not None else cond)
 
-    def feed(array, *ways, cond=None):
+    def feed(group, *ways, cond=None):
         other = 1 - q
         for way in ways:
-            if way == ACROSS:
-                send(array, me, ACROSS, across, part=q)
-            elif way == FAR:
-                send(array, me, FAR, far, part=q, cond=cond)
-            elif way == MATE:
-                send(array, me, MATE, mate, part=other, cond=cond)
-            else:
-                send(array, me, ADJACENT, adjacent, part=other, cond=inner)
-
-    def arrive(array, src, cond=None):
-        for which, size in variants(array, q):
-
-            def wait(size=size):
-                here = landing(array, src, size)
-                remote(
-                    here, here, send_sem.at[array, 0, src], recv_sem.at[array, src], {"sp": across}
-                ).wait_recv()
-
-            when(both(cond, which) if which is not None else cond, wait)
-
-    def pass_on(array, src, *ways, cond=None):
-        arrive(array, src, cond)
-        for way in ways:
-            if way == FAR:
-                send(array, src, FAR, far, cond=inner)
-            else:
-                send(array, src, ACROSS, across, cond=cond)
+            for array in group:
+                if way == ACROSS:
+                    send(array, me, ACROSS, across, part=q)
+                elif way == FAR:
+                    send(array, me, FAR, far, part=q, cond=cond)
+                elif way == MATE:
+                    send(array, me, MATE, mate, part=other, cond=cond)
+                else:
+                    send(array, me, ADJACENT, adjacent, part=other, cond=inner)
+
+    def arrive(group, src, cond=None):
+        for array in group:
+            for which, size in variants(array, q):
+
+                def wait(size=size, array=array):
+                    here = landing(array, src, size)
+                    remote(
+                        here, here, send_sem.at[array, 0], recv_sem.at[array, src], {"sp": across}
+                    ).wait_recv()
+
+                when(both(cond, which) if which is not None else cond, wait)
+
+    def pass_on(group, src, *ways, cond=None):
+        for array in group:
+            arrive((array,), src, cond)
+            for way in ways:
+                if way == FAR:
+                    send(array, src, FAR, far, cond=inner)
+                else:
+                    send(array, src, ACROSS, across, cond=cond)
 
     before = jnp.logical_and(y == 1, h == 0)
     behind = jnp.logical_and(y == 0, h == 1)
@@ -352,8 +373,7 @@
     )
 
     for way in (MATE, ADJACENT, ACROSS):
-        for array in (K, V):
-            feed(array, way)
+        feed(KEYS, way)
 
     def q_copy():
         cols = pl.ds(pl.multiple_of((1 - q) * VD, VD), VD)
@@ -376,7 +396,7 @@
     for array in (K, V):
         fetch(origin(array, q, 0), landing(array, me, 0))
     early = len(local)
-    for array in (GATE, UP, DOWN):
+    for array in GATE + UP + DOWN:
         for which, size in variants(array, q):
             fetch(origin(array, q, size), landing(array, me, size), which)
     fetch(out_weight, out_all.at[t])
@@ -451,14 +471,12 @@
         lax.fori_loop(first, last, row_block, 0)
 
     def kv_pass(src, *ways):
-        for array in (K, V):
-            pass_on(array, src, *ways)
+        pass_on(KEYS, src, *ways)
 
     per_block = length // rows
     spread_queries(q)
     attend(me, q * per_block, (q + 1) * per_block)
-    for array in (K, V):
-        feed(array, FAR)
+    feed(KEYS, FAR)
     ship(q_copy)
     ship(resid_copy(resid, t, {"sp": mate, "tp": 2 * x + q}, 2))
     feed(GATE, ACROSS)
@@ -630,7 +648,7 @@
     back = lambda: edge_copy(3, 0, begin, 1, bottom, earlier)
     ship(onward, before)
     ship(back, behind)
-    feed(DOWN, ADJACENT, FAR, MATE)
+    feed(DOWN, MATE, cond=outer)
 
     @pl.when(jnp.logical_and(y == 0, h == 0))
     def _():
@@ -643,14 +661,13 @@
     arrive(GATE, across)
     arrive(GATE, amate)
 
-    span = half_sp * depth
     wide = 2 * LANES
 
-    def expand(acc, weight, half, fresh):
-        offset = EDGE if acc is gate_acc else 0
-        held_rows = pl.ds(offset, length)
-        deep = pl.ds(pl.multiple_of(half * span, span), span)
-        blocks = pl.ds(half * half_sp, half_sp)
+    def expand(acc, weight, start, count, fresh, store=None):
+        span = count * depth
+        held_rows = pl.ds(EDGE if acc is gate_acc else 0, length)
+        deep = pl.ds(pl.multiple_of(start * depth, depth), span)
+        blocks = pl.ds(start, count)
 
         def tile(i, carry):
             b, cols = rem(i, 2), pl.ds(pl.multiple_of(div(i, 2) * wide, wide), wide)
@@ -659,7 +676,9 @@
                 weight[blocks, :, cols].reshape(span, wide),
                 preferred_element_type=f32,
             )
-            if fresh:
+            if store is not None:
+                store(b, cols, part)
+            elif fresh:
                 acc[b, held_rows, cols] = part
             else:
                 acc[b, held_rows, cols] += part
@@ -667,18 +686,21 @@
 
         lax.fori_loop(0, 2 * (big // wide), tile, 0)
 
-    expand(gate_acc, gates, h, True)
+    expand(gate_acc, gates, half_sp * h, half_sp, True)
     pass_on(UP, mate, ACROSS, cond=outer)
     arrive(GATE, afar)
     arrive(GATE, afmate)
-    expand(gate_acc, gates, 1 - h, False)
+    expand(gate_acc, gates, half_sp * (1 - h), half_sp, False)
     arrive(UP, across)
     pass_on(UP, far, ACROSS)
-    pass_on(UP, fmate, ACROSS)
+    feed(DOWN, FAR, cond=outer)
+    pass_on(UP, fmate, ACROSS, cond=inner)
     arrive(UP, amate)
-    expand(up_acc, ups, h, True)
-    pass_on(DOWN, mate, FAR)
-    send(DOWN, mate, ACROSS, across)
+    feed(DOWN, ADJACENT)
+    feed(DOWN, FAR, MATE, cond=inner)
+    expand(up_acc, ups, half_sp * h, half_sp, True)
+    pass_on(DOWN, mate, FAR, ACROSS, cond=inner)
+    pass_on(UP, fmate, ACROSS, cond=outer)
     for i in range(3):
         edge(i)().wait_recv()
     when(before, lambda: onward().wait_recv())
@@ -697,9 +719,6 @@
         return carry
 
     lax.fori_loop(0, big // wide, halo, 0)
-    arrive(UP, afar)
-    arrive(UP, afmate)
-    expand(up_acc, ups, 1 - h, False)
 
     base = jnp.where(c == q, q * (ff - big), q * (ff - small))
 
@@ -709,32 +728,33 @@
             spot = jnp.minimum(base + j * LANES, ff - LANES)
             taps = pl.ds(pl.multiple_of(spot, LANES), LANES)
 
-            def fill():
-                def tap(start):
-                    return gate_acc[b, start : start + length, cols].astype(bf16).astype(f32)
-
-                conv = (
-                    tap(EDGE - 1) * conv_weight[0:1, taps]
-                    + tap(EDGE) * conv_weight[1:2, taps]
-                    + tap(EDGE + 1) * conv_weight[2:3, taps]
-                    + conv_bias[pl.ds(div(spot, LANES), 1), :]
-                )
-                hidden[b, :, cols] = (conv / (1.0 + jnp.exp(-conv)) * up_acc[b, :, cols]).astype(
-                    bf16
-                )
-
-            if (j + 1) * LANES <= small:
-                fill()
-            else:
-                pl.when(c == q)(fill)
-
-                @pl.when(c != q)
-                def _():
-                    hidden[b, :, cols] = jnp.zeros((length, LANES), bf16)
+            def tap(start):
+                return gate_acc[b, start : start + length, cols].astype(bf16).astype(f32)
+
+            conv = (
+                tap(EDGE - 1) * conv_weight[0:1, taps]
+                + tap(EDGE) * conv_weight[1:2, taps]
+                + tap(EDGE + 1) * conv_weight[2:3, taps]
+                + conv_bias[pl.ds(div(spot, LANES), 1), :]
+            )
+            active[b, :, cols] = conv / (1.0 + jnp.exp(-conv))
 
         return carry
 
     lax.fori_loop(0, 2, activate, 0)
+    pass_on(DOWN, mate, ACROSS, cond=outer)
+    arrive(UP, afar)
+    expand(up_acc, ups, div(far, 2) * 2, 2, False)
+    arrive(UP, afmate)
+
+    def finish(b, cols, part):
+        hidden[b, :, cols] = (active[b, :, cols] * (up_acc[b, :, cols] + part)).astype(bf16)
+
+    expand(up_acc, ups, div(fmate, 2) * 2, 2, False, finish)
+
+    @pl.when(c != q)
+    def _():
+        hidden[:, :, small:] = jnp.zeros((2, length, big - small), bf16)
 
     per = sp // tp
 
@@ -759,7 +779,8 @@
 
     def x_copy(s):
         return remote(
-            stage.at[s, 1], from_x.at[rem(s, per)], part_send.at[1, s], x_recv.at[rem(s, per)],
+            stage.at[s, 1], from_x.at[rem(s, per), 0], part_send.at[1, s],
+            x_recv.at[rem(s, per)],
             {"tp": xdev},
         )
 
@@ -779,6 +800,50 @@
 
         ship(lambda: core_copy(s), c != oc)
 
+    def wide_copy(s):
+        return remote(
+            stage.at[s], from_x.at[rem(s, per)], part_send.at[0, s], x_recv.at[rem(s, per)],
+            {"tp": xdev},
+        )
+
+    def add_core_x(s):
+        ox, oc = owner(s)
+        mine = c == oc
+        slot = core_slot(s)
+
+        @pl.when(mine)
+        def _():
+            core_copy(s).wait_recv()
+
+        @pl.when(jnp.logical_and(mine, x != ox))
+        def _():
+            stage[s] = (held[slot] + from_core[slot].astype(f32)).astype(bf16)
+
+        ship(lambda: wide_copy(s), jnp.logical_and(mine, x != ox))
+
+    def add_x(s):
+        ox, oc = owner(s)
+        mine = jnp.logical_and(c == oc, x == ox)
+        slot = core_slot(s)
+
+        def summed(b):
+            return (
+                held[slot, b]
+                + from_core[slot, b].astype(f32)
+                + from_x[rem(s, per), b].astype(f32)
+            )
+
+        @pl.when(mine)
+        def _():
+            wide_copy(s).wait_recv()
+            stage[s, 0] = summed(1 - q).astype(bf16)
+
+        ship(lambda: z_copy(s), mine)
+
+        @pl.when(mine)
+        def _():
+            after_own[:, out_cols(s)] += summed(q)
+
     def add_core(s):
         ox, oc = owner(s)
         mine = c == oc
@@ -816,13 +881,14 @@
 
         ship(lambda: x_copy(s), jnp.logical_and(mine, x != ox))
 
+    settled = len(drains)
     multiply(me)
     multiply(mate)
-    add_core(me)
     pass_on(DOWN, far, ACROSS)
+    add_core_x(me)
     arrive(DOWN, across)
     multiply(across)
-    add_core(mate)
+    add_core_x(mate)
     arrive(DOWN, amate)
     multiply(amate)
     add_core(across)
@@ -830,28 +896,51 @@
     multiply(far)
     add_core(amate)
     multiply(fmate)
-    add_core(far)
+    add_core_x(far)
     when(c != q, lambda: after_copy().wait_recv())
-    add_z(me)
-    add_z(mate)
     arrive(DOWN, afar)
     multiply(afar)
-    add_core(fmate)
+    add_core_x(fmate)
+    add_x(me)
+    add_x(mate)
+    add_core(afar)
     add_z(across)
     add_z(amate)
+    for cond, make in drains[:settled]:
+        when(cond, lambda: make().wait_send())
     arrive(DOWN, afmate)
     multiply(afmate)
-    add_core(afar)
     add_core(afmate)
-    for s in (far, fmate, afar, afmate):
-        add_z(s)
+    add_x(far)
+    add_x(fmate)
+    add_z(afar)
+    add_z(afmate)
+
+    def out_copy_k(k):
+        cols = slice(k * down_cols, (k + 1) * down_cols)
+        return pltpu.make_async_copy(done.at[:, cols], out.at[:, cols], local_sem.at[16 + k])
+
     for k in range(per):
         cols = slice(k * down_cols, (k + 1) * down_cols)
-        x_copy(k).wait_recv()
-        out[:, cols] = (after_own[:, cols] + from_x[k].astype(f32)).astype(bf16)
-
-    for cond, make in drains:
+        source = per * t + k
+
+        @pl.when(y == k)
+        def _():
+            slot = core_slot(source)
+            z_copy(source).wait_recv()
+            done[:, cols] = (after_own[:, cols] + from_z[slot].astype(f32)).astype(bf16)
+
+        @pl.when(y != k)
+        def _():
+            x_copy(k).wait_recv()
+            done[:, cols] = (after_own[:, cols] + from_x[k, 0].astype(f32)).astype(bf16)
+
+        out_copy_k(k).start()
+
+    for cond, make in drains[settled:]:
         when(cond, lambda: make().wait_send())
+    for k in range(per):
+        out_copy_k(k).wait()
 
 
 def fused(sp, tp, *args):
@@ -883,7 +972,7 @@
         in_specs=[
             hbm, hbm, hbm, hbm, smem, vmem, hbm, vmem, hbm, hbm, vmem, vmem, hbm,
         ],
-        out_specs=vmem,
+        out_specs=hbm,
         scratch_shapes=[
             pltpu.VMEM((2, length, VD), bf16),
             pltpu.VMEM((maps, 2 * length, VD), bf16),
@@ -904,15 +993,17 @@
             pltpu.VMEM((2, rows, full), bf16),
             pltpu.VMEM((2, rows, big), f32),
             pltpu.VMEM((2, length, big), f32),
+            pltpu.VMEM((2, length, big), f32),
             pltpu.VMEM((2, length, big), bf16),
             pltpu.VMEM((2 * per, 2, length, down_cols), f32),
             pltpu.VMEM((sp, 2, length, down_cols), bf16),
             pltpu.VMEM((2 * per, 2, length, down_cols), bf16),
-            pltpu.VMEM((per, length, down_cols), bf16),
+            pltpu.VMEM((per, 2, length, down_cols), bf16),
             pltpu.VMEM((2 * per, length, down_cols), bf16),
-            dma((12,)),
-            dma((5, 4, sp)),
-            dma((5, sp)),
+            pltpu.VMEM(resid.shape, bf16),
+            dma((18,)),
+            dma((7, 8)),
+            dma((7, sp)),
             dma((2,)),
             dma((8,)),
             dma((heads,)),

time: 160 us -> 154 us (0.963)
  Pallas kernels: 158 us -> 151 us
    pallas_call x1, Pallas kernels: 158 us -> 151 us  [fused(): pl.pallas_call(functools.partial(layer_kernel, sp, tp), out_shape=jax.Sha...]
where the time goes in v4:
time: 154 us; the launch traced here: 153 us
  Pallas kernels  151 us (98%)
  local copies, waits for them, and re-layouts  1.87 us (1%)
    pallas_call x1, Pallas kernels, fused(): pl.pallas_call(functools.partial(layer_kernel, sp, tp), out_shape=jax.Sha...  151 us

profile of v4, /device:TPU:0, one launch (start us, length us, event | category | flops | bytes accessed | tf_op | source)
XLA Modules:
  0.0 152.5 jit_solution(2441522521859680100)
XLA Ops:
  0.0 150.6 %shard_map.127 = bf16[512,512]{1,0:T(8,128)(2,1)} custom-call(bf16[512,512]{1,0:T(8,128)(2,1)} %resid.1, bf16[512,256]{1,0:T(8,128)(2,1)} %queries.1, bf16[512,256]{1,0:T(8,128)(2,1)} %keys.1, bf16[512,256]{1,0:T(8,128)(2,1)} %values.1, f32[2]{0:T(128)} %mix_lambda.1, f32[1,128]{1,0:T(1,128)} %bitcast.5, bf16[1024,512]{1,0:T(8,128)(2,1)} %out_weight.1, ...), custom_call_target="tpu_custom_call" | custom-call | tf_op jit(solution)/shard_map/pallas_call | solution.py:969
  150.6 1.9 %copy.15 = bf16[512,512]{1,0:T(8,128)(2,1)} copy(bf16[512,512]{1,0:T(8,128)(2,1)} %shard_map.127) | data formatting | bytes 1048576

commit v5 on v4

--- a/solution.py
+++ b/solution.py
@@ -177,7 +177,6 @@
     from_core,
     from_x,
     from_z,
-    done,
     local_sem,
     send_sem,
     recv_sem,
@@ -884,19 +883,21 @@
     settled = len(drains)
     multiply(me)
     multiply(mate)
-    pass_on(DOWN, far, ACROSS)
+    pass_on(DOWN, far, ACROSS, cond=inner)
+    pass_on(DOWN[:1], far, ACROSS, cond=outer)
     add_core_x(me)
     arrive(DOWN, across)
     multiply(across)
+    pass_on(DOWN[1:], far, ACROSS, cond=outer)
     add_core_x(mate)
     arrive(DOWN, amate)
     multiply(amate)
     add_core(across)
-    pass_on(DOWN, fmate, ACROSS)
     multiply(far)
     add_core(amate)
+    add_core_x(far)
+    pass_on(DOWN, fmate, ACROSS)
     multiply(fmate)
-    add_core_x(far)
     when(c != q, lambda: after_copy().wait_recv())
     arrive(DOWN, afar)
     multiply(afar)
@@ -915,11 +916,8 @@
     add_x(fmate)
     add_z(afar)
     add_z(afmate)
-
-    def out_copy_k(k):
-        cols = slice(k * down_cols, (k + 1) * down_cols)
-        return pltpu.make_async_copy(done.at[:, cols], out.at[:, cols], local_sem.at[16 + k])
-
+    for cond, make in drains[settled:]:
+        when(cond, lambda: make().wait_send())
     for k in range(per):
         cols = slice(k * down_cols, (k + 1) * down_cols)
         source = per * t + k
@@ -928,19 +926,12 @@
         def _():
             slot = core_slot(source)
             z_copy(source).wait_recv()
-            done[:, cols] = (after_own[:, cols] + from_z[slot].astype(f32)).astype(bf16)
+            out[:, cols] = (after_own[:, cols] + from_z[slot].astype(f32)).astype(bf16)
 
         @pl.when(y != k)
         def _():
             x_copy(k).wait_recv()
-            done[:, cols] = (after_own[:, cols] + from_x[k, 0].astype(f32)).astype(bf16)
-
-        out_copy_k(k).start()
-
-    for cond, make in drains[settled:]:
-        when(cond, lambda: make().wait_send())
-    for k in range(per):
-        out_copy_k(k).wait()
+            out[:, cols] = (after_own[:, cols] + from_x[k, 0].astype(f32)).astype(bf16)
 
 
 def fused(sp, tp, *args):
@@ -968,11 +959,11 @@
     args[11] = args[11].reshape(-1, LANES)
     return pl.pallas_call(
         functools.partial(layer_kernel, sp, tp),
-        out_shape=jax.ShapeDtypeStruct(resid.shape, bf16),
+        out_shape=pltpu.VMEM(resid.shape, bf16),
         in_specs=[
             hbm, hbm, hbm, hbm, smem, vmem, hbm, vmem, hbm, hbm, vmem, vmem, hbm,
         ],
-        out_specs=hbm,
+        out_specs=vmem,
         scratch_shapes=[
             pltpu.VMEM((2, length, VD), bf16),
             pltpu.VMEM((maps, 2 * length, VD), bf16),
@@ -1000,8 +991,7 @@
             pltpu.VMEM((2 * per, 2, length, down_cols), bf16),
             pltpu.VMEM((per, 2, length, down_cols), bf16),
             pltpu.VMEM((2 * per, length, down_cols), bf16),
-            pltpu.VMEM(resid.shape, bf16),
-            dma((18,)),
+            dma((16,)),
             dma((7, 8)),
             dma((7, sp)),
             dma((2,)),

time: 154 us -> 152 us (0.987)
  no operation moved by 1% of the time
where the time goes in v5:
time: 152 us
  Pallas kernels  151 us (99%)
    pallas_call x1, Pallas kernels, fused(): pl.pallas_call(functools.partial(layer_kernel, sp, tp), out_shape=pltpu.V...  151 us

profile of v5, /device:TPU:0, one launch (start us, length us, event | category | flops | bytes accessed | tf_op | source)
XLA Modules:
  0.0 151.5 jit_solution(6586583115105966270)
XLA Ops:
  0.0 150.7 %shard_map.127 = bf16[512,512]{1,0:T(8,128)(2,1)S(1)} custom-call(bf16[512,512]{1,0:T(8,128)(2,1)} %resid.1, bf16[512,256]{1,0:T(8,128)(2,1)} %queries.1, bf16[512,256]{1,0:T(8,128)(2,1)} %keys.1, bf16[512,256]{1,0:T(8,128)(2,1)} %values.1, f32[2]{0:T(128)} %mix_lambda.1, f32[1,128]{1,0:T(1,128)} %bitcast.5, bf16[1024,512]{1,0:T(8,128)(2,1)} %out_weight.1, ...), custom_call_target="tpu_custom_call" | custom-call | tf_op jit(solution)/shard_map/pallas_call | solution.py:960
  150.7 0.8 copy.15

commit v6 on v5

--- a/solution.py
+++ b/solution.py
@@ -695,9 +695,11 @@
     feed(DOWN, FAR, cond=outer)
     pass_on(UP, fmate, ACROSS, cond=inner)
     arrive(UP, amate)
-    feed(DOWN, ADJACENT)
-    feed(DOWN, FAR, MATE, cond=inner)
+    feed(DOWN, MATE, cond=inner)
     expand(up_acc, ups, half_sp * h, half_sp, True)
+    for piece in DOWN:
+        feed((piece,), FAR, cond=inner)
+        feed((piece,), ADJACENT)
     pass_on(DOWN, mate, FAR, ACROSS, cond=inner)
     pass_on(UP, fmate, ACROSS, cond=outer)
     for i in range(3):
@@ -741,7 +743,6 @@
         return carry
 
     lax.fori_loop(0, 2, activate, 0)
-    pass_on(DOWN, mate, ACROSS, cond=outer)
     arrive(UP, afar)
     expand(up_acc, ups, div(far, 2) * 2, 2, False)
     arrive(UP, afmate)
@@ -882,6 +883,7 @@
 
     settled = len(drains)
     multiply(me)
+    pass_on(DOWN, mate, ACROSS, cond=outer)
     multiply(mate)
     pass_on(DOWN, far, ACROSS, cond=inner)
     pass_on(DOWN[:1], far, ACROSS, cond=outer)

time: 152 us -> 151 us (level)
  Pallas kernels: 151 us -> 149 us
    pallas_call x1, Pallas kernels: 151 us -> 149 us  [fused(): pl.pallas_call(functools.partial(layer_kernel, sp, tp), out_shape=pltpu.V...]
where the time goes in v6:
time: 151 us; the launch traced here: 150 us
  Pallas kernels  149 us (99%)
    pallas_call x1, Pallas kernels, fused(): pl.pallas_call(functools.partial(layer_kernel, sp, tp), out_shape=pltpu.V...  149 us

profile of v6, /device:TPU:0, one launch (start us, length us, event | category | flops | bytes accessed | tf_op | source)
XLA Modules:
  0.0 149.6 jit_solution(10701050605430318182)
XLA Ops:
  0.0 148.8 %shard_map.127 = bf16[512,512]{1,0:T(8,128)(2,1)S(1)} custom-call(bf16[512,512]{1,0:T(8,128)(2,1)} %resid.1, bf16[512,256]{1,0:T(8,128)(2,1)} %queries.1, bf16[512,256]{1,0:T(8,128)(2,1)} %keys.1, bf16[512,256]{1,0:T(8,128)(2,1)} %values.1, f32[2]{0:T(128)} %mix_lambda.1, f32[1,128]{1,0:T(1,128)} %bitcast.5, bf16[1024,512]{1,0:T(8,128)(2,1)} %out_weight.1, ...), custom_call_target="tpu_custom_call" | custom-call | tf_op jit(solution)/shard_map/pallas_call | solution.py:962
  148.8 0.8 copy.15
